TPU v7x, 32 devices: a whole 2x2x4 slice. The times are simulated.
32 devices in a mesh: grp: 2 (over y), ep: 8 (over z, x), tp: 2 (over core).
Axes of the slice: x: 2, y: 2, z: 4, core: 2. Of those that a mesh axis runs over, the one named last changes fastest.
Arguments:
- fresh_inputs: bfloat16 [256, 2048], P(('grp', 'ep')), parts along dimension 0, may hold values from -6 to 6
- memory_arrays: float32 [256, 32, 64, 64], P(('grp', 'ep'), 'tp'), parts along dimension 0, may hold values from -4 to 4
- chosen_specialist: int32 [256, 2], P(('grp', 'ep')), parts along dimension 0, may hold values from 0 to 3, all different within a row; in each aligned block of 128 rows (0 to 127, 128 to 255, ...) at most 96 rows name the same one
- chosen_coefficient: bfloat16 [256, 2], P(('grp', 'ep')), parts along dimension 0, may hold values from 0.25 to 1
- first_rescale: float32 [2048], replicated, may hold values from 0.1 to 1.9
- second_rescale: float32 [2048], replicated, may hold values from 0.1 to 1.9
- receiver_projector: bfloat16 [2048, 2048], P('tp', 'ep'), may hold values from -0.125 to 0.125
- address_projector: bfloat16 [2048, 2048], P('tp', 'ep'), may hold values from -0.125 to 0.125
- content_projector: bfloat16 [2048, 2048], P('tp', 'ep'), may hold values from -0.125 to 0.125
- final_projector: bfloat16 [2048, 2048], P('tp', 'ep'), may hold values from -0.125 to 0.125
- forget_narrowing: bfloat16 [2048, 64], replicated, may hold values from -0.125 to 0.125
- forget_widening: bfloat16 [64, 2048], P(None, 'tp'), may hold values from -0.75 to 0.75
- forget_bias: float32 [2048], P('tp'), may hold values from -3 to 1
- learning_narrowing: bfloat16 [2048, 64], replicated, may hold values from -0.125 to 0.125
- learning_widening: bfloat16 [64, 2048], P(None, 'tp'), may hold values from -0.75 to 0.75
- learning_bias: float32 [2048], P('tp'), may hold values from -1.5 to 1.5
- lane_scaling: float32 [2048], P('tp'), may hold values from 0.1 to 1.9
- instant_reward: float32 [32, 64], P('tp'), may hold values from -0.5 to 0.5
- specialist_switch: bfloat16 [2048, 28672], P(None, ('ep', 'tp')), may hold values from -0.125 to 0.125
- specialist_expand: bfloat16 [2048, 28672], P(None, ('ep', 'tp')), may hold values from -0.125 to 0.125
- specialist_contract: bfloat16 [28672, 2048], P(('ep', 'tp')), may hold values from -0.0625 to 0.0625
- common_activator: bfloat16 [2048, 5632], P(None, ('ep', 'tp')), may hold values from -0.125 to 0.125
- common_expand: bfloat16 [2048, 5632], P(None, ('ep', 'tp')), may hold values from -0.125 to 0.125
- common_contract: bfloat16 [5632, 2048], P(('ep', 'tp')), may hold values from -0.078125 to 0.078125
- common_switch: bfloat16 [2048], replicated, may hold values from -0.125 to 0.125
Outputs:
- new_tokens: bfloat16 [256, 2048], P(('grp', 'ep', 'tp')), parts along dimension 0
- memory_after: float32 [256, 32, 64, 64], P(('grp', 'ep'), 'tp'), parts along dimension 0
There are 2 independent parts, one for each index of `grp`. A program takes and returns all parts, laid end to end along the dimension named above; an argument that names none is the same for every part. Nothing has to cross between parts.
Inputs may be any that keep to these rules, and one draw needn't show every extreme that they name: `chosen_specialist`: each row names 2 different experts. Over the whole batch no expert is named by more than 96 rows, and in every draw some expert is named by exactly 96 rows.
All inputs are finite; a program needn't handle non-finite values.
Results may differ from a plain program's by a relative error of at most 0.014.
Values may be sent and summed in bfloat16 or wider, within the bound.
A program may use at most 128 MiB of HBM per device.

v0:
```python
import jax
import jax.numpy as jnp
from jax import lax
from jax.sharding import PartitionSpec as P

LANE_WIDTH = 64
FF_E = 7168


RMS_EPS = 1e-06
GROUP_EPS = 0.00064
HIGHEST = lax.Precision.HIGHEST


def rms_norm(values, norm_gain):
    mean_sq = jnp.mean(values * values, axis=-1, keepdims=True)
    return values * lax.rsqrt(mean_sq + RMS_EPS) * norm_gain


def widen(rounded):
    return lax.optimization_barrier(rounded).astype(jnp.float32)


def evolve_memory(
    memory_arrays,
    receiver_lanes,
    address_lanes,
    content_lanes,
    forget_lanes,
    learning_lanes,
    lane_rescale,
    instant_reward,
):
    unit_key = address_lanes * lax.rsqrt(
        jnp.sum(address_lanes * address_lanes, axis=-1, keepdims=True) + 1.0
    )
    stepped_address = address_lanes * learning_lanes
    removal = jnp.einsum("bhvk,bhk->bhv", memory_arrays, unit_key, precision=HIGHEST)
    memory_after = (
        memory_arrays * forget_lanes[:, :, None, :]
        - removal[..., None] * (unit_key * learning_lanes)[:, :, None, :]
        + content_lanes[..., None] * stepped_address[:, :, None, :]
    )
    memory_retrieval = jnp.einsum("bhvk,bhk->bhv", memory_after, receiver_lanes, precision=HIGHEST)
    centred = memory_retrieval - jnp.mean(memory_retrieval, axis=-1, keepdims=True)
    unit_address = centred * lax.rsqrt(
        jnp.mean(centred * centred, axis=-1, keepdims=True) + GROUP_EPS
    )
    instant_extra = (
        jnp.sum(receiver_lanes * stepped_address * instant_reward, axis=-1, keepdims=True)
        * content_lanes
    )
    return (memory_after, unit_address * lane_rescale + instant_extra)


def swiglu(rows_in, gate_w, up_w):
    gate_val = jnp.dot(rows_in, gate_w, preferred_element_type=jnp.float32)
    up_val = jnp.dot(rows_in, up_w, preferred_element_type=jnp.float32)
    return (jax.nn.silu(gate_val) * up_val).astype(jnp.bfloat16)


def body(
    fresh_inputs,
    memory_arrays,
    chosen_specialist,
    chosen_coefficient,
    first_rescale,
    second_rescale,
    receiver_projector,
    address_projector,
    content_projector,
    final_projector,
    forget_narrowing,
    forget_widening,
    forget_bias,
    learning_narrowing,
    learning_widening,
    learning_bias,
    lane_scaling,
    instant_reward,
    specialist_switch,
    specialist_expand,
    specialist_contract,
    common_activator,
    common_expand,
    common_contract,
    common_switch,
):
    own_rows = fresh_inputs.shape[0]
    model_width = fresh_inputs.shape[1]
    tp_count = lax.axis_size("tp")
    tp_rank = lax.axis_index("tp")
    half_width = model_width // tp_count
    head_count = half_width // LANE_WIDTH
    residual = fresh_inputs.astype(jnp.float32)
    normed = rms_norm(residual, first_rescale).astype(jnp.bfloat16)
    normed_half = lax.dynamic_slice_in_dim(normed, tp_rank * half_width, half_width, 1)
    local_weights = jnp.stack((receiver_projector, address_projector, content_projector), axis=1)
    projected_rows = jnp.einsum(
        "rd,dkc->rkc",
        lax.all_gather(normed_half, "ep", axis=0, tiled=True),
        local_weights,
        preferred_element_type=jnp.float32,
    ).astype(jnp.bfloat16)
    partial_value = lax.all_to_all(projected_rows, "ep", split_axis=0, concat_axis=2, tiled=True)
    projected = lax.psum(widen(partial_value).astype(jnp.bfloat16), "tp")
    mine = lax.dynamic_slice_in_dim(projected, tp_rank * half_width, half_width, 2)

    def divide_lanes(channels):
        return channels.astype(jnp.float32).reshape(own_rows, head_count, LANE_WIDTH)

    decay_mid = jnp.tanh(
        jnp.dot(normed, forget_narrowing, preferred_element_type=jnp.float32)
    ).astype(jnp.bfloat16)
    decay_pre = forget_bias + jnp.dot(
        decay_mid, forget_widening, preferred_element_type=jnp.float32
    )
    decay_vals = jnp.exp(-jnp.exp(-jax.nn.softplus(-decay_pre) - 0.5))
    rate_mid = jnp.dot(normed, learning_narrowing, preferred_element_type=jnp.float32).astype(
        jnp.bfloat16
    )
    rate_vals = jax.nn.sigmoid(
        learning_bias + jnp.dot(rate_mid, learning_widening, preferred_element_type=jnp.float32)
    )
    memory_after, memory_retrieval = evolve_memory(
        memory_arrays,
        divide_lanes(mine[:, 0]),
        divide_lanes(mine[:, 1]),
        divide_lanes(mine[:, 2]),
        divide_lanes(decay_vals),
        divide_lanes(rate_vals),
        lane_scaling.reshape(head_count, LANE_WIDTH),
        instant_reward,
    )
    attended = memory_retrieval.reshape(own_rows, half_width).astype(jnp.bfloat16)
    done_rows = jnp.dot(
        lax.all_gather(attended, "ep", axis=0, tiled=True),
        final_projector,
        preferred_element_type=jnp.float32,
    ).astype(jnp.bfloat16)
    out_part = lax.all_to_all(done_rows, "ep", split_axis=0, concat_axis=1, tiled=True)
    mixed_out = lax.psum(widen(out_part).astype(jnp.bfloat16), "tp")
    residual = residual + mixed_out.astype(jnp.float32)
    ffn_in = rms_norm(residual, second_rescale).astype(jnp.bfloat16)
    all_in, all_weight, all_ids = (
        lax.all_gather(ffn_in, "ep", axis=0, tiled=True),
        lax.all_gather(chosen_coefficient, "ep", axis=0, tiled=True),
        lax.all_gather(chosen_specialist, "ep", axis=0, tiled=True),
    )
    column_count = specialist_switch.shape[1]
    flat_rank = lax.axis_index("ep") * tp_count + tp_rank
    expert = flat_rank * column_count // FF_E
    expert_share = jnp.sum(
        jnp.where(all_ids == expert, all_weight.astype(jnp.float32), 0.0), axis=1
    )
    hidden = swiglu(all_in, specialist_switch, specialist_expand)
    shared_hidden = swiglu(all_in, common_activator, common_expand)
    branch_scale = jax.nn.sigmoid(
        jnp.dot(all_in, common_switch, preferred_element_type=jnp.float32)
    )
    rows_mine = own_rows // tp_count
    expert_term = expert_share[:, None] * jnp.dot(
        hidden, specialist_contract, preferred_element_type=jnp.float32
    )
    routed = lax.psum_scatter(
        expert_term
        + branch_scale[:, None]
        * jnp.dot(shared_hidden, common_contract, preferred_element_type=jnp.float32),
        ("ep", "tp"),
        scatter_dimension=0,
        tiled=True,
    )
    own_residual = lax.dynamic_slice_in_dim(residual, tp_rank * rows_mine, rows_mine, 0)
    return ((own_residual + routed).astype(jnp.bfloat16), memory_after)


def solution(mesh):
    placed = (
        P(("grp", "ep"), None),
        P(("grp", "ep"), "tp", None, None),
        P(("grp", "ep"), None),
        P(("grp", "ep"), None),
        P(),
        P(),
        P("tp", "ep"),
        P("tp", "ep"),
        P("tp", "ep"),
        P("tp", "ep"),
        P(),
        P(None, "tp"),
        P("tp"),
        P(),
        P(None, "tp"),
        P("tp"),
        P("tp"),
        P("tp", None),
        P(None, ("ep", "tp")),
        P(None, ("ep", "tp")),
        P(("ep", "tp"), None),
        P(None, ("ep", "tp")),
        P(None, ("ep", "tp")),
        P(("ep", "tp"), None),
        P(),
    )
    return jax.shard_map(
        body,
        mesh=mesh,
        in_specs=placed,
        out_specs=(P(("grp", "ep", "tp"), None), P(("grp", "ep"), "tp", None, None)),
        check_vma=False,
    )
```

profile of v0, /device:TPU:0, one launch (start us, length us, event | category | flops | bytes accessed | tf_op | source)
XLA Modules:
  0.0 324.2 jit_solution(6716720031161532944)
XLA Ops:
  7.2 0.0 copy-start
  7.2 0.0 copy-start.6
  7.2 0.0 copy-start.7
  7.2 0.0 copy-start.10
  7.2 0.0 copy-start.11
  7.2 1.1 fusion.33
  8.3 0.9 fusion.35
  9.3 32.6 %all_gather.15 = bf16[128,1024]{1,0:T(8,128)(2,1)S(1)} all-gather(bf16[16,1024]{1,0:T(8,128)(2,1)S(1)} %constant_dynamic-slice_fusion.1), channel_id=1, replica_groups=mesh['grp'=2,'ep'=8,'tp'=2] {'ep'}, dimensions={0}, use_global_device_ids=true | all-gather | bytes 294912 | tf_op jit(solution)/shard_map/all_gather | solution.py:101
  41.8 1.7 fusion.9
  43.6 0.9 copy.30
  44.5 5.5 %all-to-all-start = ((bf16[128,3,256]{2,1,0:T(4,128)(2,1)}), bf16[128,3,256]{2,1,0:T(4,128)(2,1)S(1)}, u32[]{:S(2)}, u32[]{:S(2)}) async-start(bf16[128,3,256]{2,1,0:T(4,128)(2,1)} %copy.30), calls=%async_computation | async-start | bytes 524288 | tf_op jit(solution)/shard_map/all_to_all | solution.py:105
  50.0 0.0 all-reduce.3.cloned.1.call-start
  50.0 1.4 fusion.19
  51.4 0.1 reshape.102
  51.5 6.7 %all-to-all-done = bf16[128,3,256]{2,1,0:T(4,128)(2,1)S(1)} async-done(((bf16[128,3,256]{2,1,0:T(4,128)(2,1)}), bf16[128,3,256]{2,1,0:T(4,128)(2,1)S(1)}, u32[]{:S(2)}, u32[]{:S(2)}) %all-to-all-start) | async-done | bytes 196640 | tf_op jit(solution)/shard_map/all_to_all | solution.py:105
  58.2 0.1 copy.39
  58.3 0.8 all_to_all.30
  59.1 0.0 all-reduce.3.cloned.1.call-update
  59.2 0.4 fusion.42
  59.6 0.1 mul.207
  59.7 0.1 mul.225
  59.7 15.9 %all-reduce.3.cloned.1.call-done = bf16[16,3,2048]{2,0,1:T(8,128)(2,1)} async-done(((bf16[16,3,2048]{2,0,1:T(8,128)(2,1)}), bf16[16,3,2048]{2,0,1:T(8,128)(2,1)}) %all-reduce.3.cloned.1.call-update) | async-done | bytes 196624 | tf_op jit(solution)/shard_map/psum | solution.py:106
  75.7 0.8 constant_dynamic-slice_fusion
  76.5 0.1 reshape.124
  76.6 0.1 reshape.103
  76.7 0.1 reshape.104
  76.8 0.1 multiply_reduce_fusion.2
  76.9 0.1 reshape.105
  77.0 0.1 fusion.48
  77.1 15.4 %fusion.49 = f32[16,16,1,64]{3,2,1,0:T(1,128)S(1)} fusion(f32[16,16,64,1]{2,3,1,0:T(1,128)S(1)} %bitcast.75, f32[16,16,64,64]{3,2,1,0:T(8,128)} %param.26), kind=kOutput, calls=%fused_computation.80 | convolution fusion | flops 12582912 | bytes 4325376 | tf_op jit(solution)/shard_map/bhvk,bhk->bhv/dot_general | solution.py:38
  92.5 8.6 %multiply_add_fusion = f32[16,16,64,64]{3,2,1,0:T(8,128)S(1)} fusion(f32[16,16,64,64]{3,2,1,0:T(8,128)} %param.26, f32[16,16,64]{2,1,0:T(8,128)S(1)} %get-tuple-element.4, f32[16,16,64]{2,1,0:T(8,128)S(1)} %reshape.105, f32[16,16,64]{2,1,0:T(8,128)S(1)} %get-tuple-element.2, f32[16,16,64]{2,1,0:T(8,128)S(1)} %bitcast.74, f32[16,16,64]{2,1,0:T(8,128)S(1)} %mul.207), kind=kLoop, calls=%fused_computation.1 | loop fusion | flops 5242880 | bytes 8716288 | tf_op jit(solution)/shard_map/add | solution.py:40
  101.1 0.0 copy-start.1
  101.1 3.4 %copy-done.1 = f32[16,16,64,64]{3,2,1,0:T(8,128)} copy-done((f32[16,16,64,64]{3,2,1,0:T(8,128)}, f32[16,16,64,64]{3,2,1,0:T(8,128)S(1)}, u32[]{:S(2)}) %copy-start.1) | copy-done | bytes 4194328
  104.5 0.0 copy-start.12
  104.5 0.0 copy-start.4
  104.5 0.0 copy-start.9
  104.6 6.6 %fusion.50 = f32[16,16,1,64]{3,2,1,0:T(1,128)S(1)} fusion(f32[16,16,64,64]{3,2,1,0:T(8,128)S(1)} %multiply_add_fusion, bf16[16,16,64,1]{2,3,1,0:T(2,128)(2,1)S(1)} %reshape.124), kind=kOutput, calls=%fused_computation.81 | convolution fusion | flops 12582912 | bytes 4292608 | tf_op jit(solution)/shard_map/bhvk,bhk->bhv/dot_general | solution.py:44
  111.2 0.1 reduce_sum.65
  111.3 0.2 multiply_reduce_fusion.1
  111.5 0.5 fusion.15
  112.0 0.1 convert_element_type.98
  112.2 31.1 %all_gather.16 = bf16[128,1024]{1,0:T(8,128)(2,1)S(1)} all-gather(bf16[16,1024]{1,0:T(8,128)(2,1)S(1)} %convert_element_type.98), channel_id=1, replica_groups=mesh['grp'=2,'ep'=8,'tp'=2] {'ep'}, dimensions={0}, use_global_device_ids=true | all-gather | bytes 294912 | tf_op jit(solution)/shard_map/all_gather | solution.py:137
  143.3 0.8 convolution_convert_fusion
  144.1 5.4 %all-to-all-start.1 = ((bf16[8,16,256]{2,1,0:T(8,128)(2,1)}), bf16[8,16,256]{2,1,0:T(8,128)(2,1)S(1)}, u32[]{:S(2)}, u32[]{:S(2)}) async-start(bf16[8,16,256]{2,1,0:T(8,128)(2,1)} %bitcast.12), calls=%async_computation.1 | async-start | bytes 131072 | tf_op jit(solution)/shard_map/all_to_all | solution.py:141
  149.6 0.0 all-reduce.5.cloned.1.call-start
  149.6 20.9 %all-gather.1 = bf16[8,16,2]{1,2,0:T(2,128)(2,1)S(1)} all-gather(bf16[1,16,2]{1,2,0:T(2,128)(2,1)S(1)} %bitcast.79), channel_id=1, replica_groups=mesh['grp'=2,'ep'=8,'tp'=2] {'ep'}, dimensions={0}, use_global_device_ids=true | all-gather | bytes 576 | tf_op jit(solution)/shard_map/all_gather | solution.py:147
  170.6 16.5 %all-gather = s32[8,16,2]{1,2,0:T(2,128)S(1)} all-gather(s32[1,16,2]{1,2,0:T(2,128)S(1)} %bitcast.78), channel_id=1, replica_groups=mesh['grp'=2,'ep'=8,'tp'=2] {'ep'}, dimensions={0}, use_global_device_ids=true | all-gather | bytes 1152 | tf_op jit(solution)/shard_map/all_gather | solution.py:148
  187.0 0.0 all-to-all-done.1
  187.0 0.6 copy.37
  187.6 0.0 all-reduce.5.cloned.1.call-update
  187.7 0.0 reduce-scatter.2.cloned.1.call-start
  187.7 0.1 reshape.115
  187.8 16.4 %all-reduce.5.cloned.1.call-done = bf16[16,2048]{1,0:T(8,128)(2,1)} async-done(((bf16[16,2048]{1,0:T(8,128)(2,1)}), bf16[16,2048]{1,0:T(8,128)(2,1)}) %all-reduce.5.cloned.1.call-update) | async-done | bytes 65552 | tf_op jit(solution)/shard_map/psum | solution.py:142
  204.2 1.0 convert_add_fusion
  205.2 0.9 multiply_convert_fusion
  206.1 31.8 %all_gather.19 = bf16[128,2048]{1,0:T(8,128)(2,1)S(1)} all-gather(bf16[16,2048]{1,0:T(8,128)(2,1)S(1)} %multiply_convert_fusion), channel_id=1, replica_groups=mesh['grp'=2,'ep'=8,'tp'=2] {'ep'}, dimensions={0}, use_global_device_ids=true | all-gather | bytes 589824 | tf_op jit(solution)/shard_map/all_gather | solution.py:146
  237.9 5.3 %fusion.51 = f32[128,1792]{1,0:T(8,128)} fusion(bf16[128,2048]{1,0:T(8,128)(2,1)S(1)} %all_gather.19, bf16[2048,1792]{1,0:T(8,128)(2,1)} %param.43), kind=kOutput, calls=%fused_computation.82 | convolution fusion | flops 939524096 | bytes 8781824 | tf_op jit(solution)/shard_map/dot_general | solution.py:57
  243.2 1.2 fusion.52
  244.4 0.2 fusion.25
  244.7 9.1 %convolution_multiply_fusion.1 = f32[128,2048]{1,0:T(8,128)} fusion(bf16[1792,2048]{1,0:T(8,128)(2,1)} %param.45, bf16[128,2048]{1,0:T(8,128)(2,1)S(1)} %all_gather.19, bf16[2048,1792]{1,0:T(8,128)(2,1)} %param.44, f32[128,1792]{1,0:T(8,128)} %fusion.51, f32[128]{0:T(128)S(1)} %reshape.115), kind=kOutput, calls=%fused_computation.3 | convolution fusion | flops 1880686592 | bytes 17170944 | tf_op jit(solution)/shard_map/dot_general | solution.py:162
  253.7 3.8 %fusion.1 = f32[128,2048]{1,0:T(8,128)} fusion(f32[128,2048]{1,0:T(8,128)} %convolution_multiply_fusion.1, bf16[352,2048]{1,0:T(8,128)(2,1)S(1)} %copy-done, bf16[128,2048]{1,0:T(8,128)(2,1)S(1)} %all_gather.19, bf16[2048,352]{0,1:T(8,128)(2,1)S(1)} %copy-done.3, f32[128]{0:T(128)S(1)} %fusion.25, f32[128,352]{0,1:T(8,128)} %fusion.52), kind=kOutput, calls=%fused_computation.5 | convolution fusion | flops 369893376 | bytes 5685760 | tf_op jit(solution)/shard_map/dot_general | solution.py:168
  257.5 0.0 reduce-scatter.2.cloned.1.call-update
  257.6 58.6 %reduce-scatter.2.cloned.1.call-done = f32[8,2048]{1,0:T(8,128)} async-done(((f32[128,2048]{1,0:T(8,128)}), f32[8,2048]{1,0:T(8,128)}) %reduce-scatter.2.cloned.1.call-update) | async-done | bytes 65552 | tf_op jit(solution)/shard_map/reduce_scatter | solution.py:165
  316.2 1.5 add_convert_fusion
  (28 shorter events, 0.1 us)
Async XLA Ops:
  7.2 246.6 %copy-start = (bf16[352,2048]{1,0:T(8,128)(2,1)S(1)}, bf16[352,2048]{1,0:T(8,128)(2,1)}, u32[]{:S(2)}) copy-start(bf16[352,2048]{1,0:T(8,128)(2,1)} %param.48) | copy-start | bytes 4325380
  7.2 52.0 %copy-start.6 = (bf16[2048,64]{0,1:T(8,128)(2,1)S(1)}, bf16[2048,64]{0,1:T(8,128)(2,1)}, u32[]{:S(2)}) copy-start(bf16[2048,64]{0,1:T(8,128)(2,1)} %param.35) | copy-start | bytes 786436
  7.2 52.0 %copy-start.7 = (bf16[64,1024]{1,0:T(8,128)(2,1)S(1)}, bf16[64,1024]{1,0:T(8,128)(2,1)}, u32[]{:S(2)}) copy-start(bf16[64,1024]{1,0:T(8,128)(2,1)} %param.36) | copy-start | bytes 393220
  7.2 52.0 %copy-start.10 = (f32[1024]{0:T(1024)S(1)}, f32[1024]{0:T(1024)}, u32[]{:S(2)}) copy-start(f32[1024]{0:T(1024)} %param.37) | copy-start | bytes 12292
  7.2 52.5 %copy-start.11 = (f32[1024]{0:T(1024)S(1)}, f32[1024]{0:T(1024)}, u32[]{:S(2)}) copy-start(f32[1024]{0:T(1024)} %param.41) | copy-start | bytes 12292
  44.5 13.7 %all-to-all-start = ((bf16[128,3,256]{2,1,0:T(4,128)(2,1)}), bf16[128,3,256]{2,1,0:T(4,128)(2,1)S(1)}, u32[]{:S(2)}, u32[]{:S(2)}) async-start(bf16[128,3,256]{2,1,0:T(4,128)(2,1)} %copy.30), calls=%async_computation | async-start | bytes 524288 | tf_op jit(solution)/shard_map/all_to_all | solution.py:105
  50.0 25.7 %all-reduce.3.cloned.1.call-start = ((), (), s32[]{:S(2)}) async-start(), calls=%async_computation.3 | async-start | bytes 393216 | tf_op jit(solution)/shard_map/psum | solution.py:106
  101.1 3.4 %copy-start.1 = (f32[16,16,64,64]{3,2,1,0:T(8,128)}, f32[16,16,64,64]{3,2,1,0:T(8,128)S(1)}, u32[]{:S(2)}) copy-start(f32[16,16,64,64]{3,2,1,0:T(8,128)S(1)} %multiply_add_fusion) | copy-start | bytes 12582916
  104.5 7.0 %copy-start.8 = (f32[16,64]{1,0:T(8,128)S(1)}, f32[16,64]{1,0:T(8,128)}, u32[]{:S(2)}) copy-start(f32[16,64]{1,0:T(8,128)} %param.42) | copy-start | bytes 12292
  104.5 38.8 %copy-start.5 = (bf16[1024,256]{1,0:T(8,128)(2,1)S(1)}, bf16[1024,256]{1,0:T(8,128)(2,1)}, u32[]{:S(2)}) copy-start(bf16[1024,256]{1,0:T(8,128)(2,1)} %param.34) | copy-start | bytes 1572868
  104.5 45.1 %copy-start.14 = (bf16[16,2]{0,1:T(2,128)(2,1)S(1)}, bf16[16,2]{0,1:T(2,128)(2,1)}, u32[]{:S(2)}) copy-start(bf16[16,2]{0,1:T(2,128)(2,1)} %param.28) | copy-start | bytes 196
  104.5 66.0 %copy-start.13 = (s32[16,2]{0,1:T(2,128)S(1)}, s32[16,2]{0,1:T(2,128)}, u32[]{:S(2)}) copy-start(s32[16,2]{0,1:T(2,128)} %param.27) | copy-start | bytes 388
  104.5 83.3 %copy-start.12 = (bf16[2048]{0:T(1024)(128)(2,1)S(1)}, bf16[2048]{0:T(1024)(128)(2,1)}, u32[]{:S(2)}) copy-start(bf16[2048]{0:T(1024)(128)(2,1)} %param.49) | copy-start | bytes 12292
  104.5 99.7 %copy-start.4 = (bf16[16,2048]{1,0:T(8,128)(2,1)S(1)}, bf16[16,2048]{1,0:T(8,128)(2,1)}, u32[]{:S(2)}) copy-start(bf16[16,2048]{1,0:T(8,128)(2,1)} %param.25) | copy-start | bytes 196612
  104.5 100.7 %copy-start.9 = (f32[2048]{0:T(1024)S(1)}, f32[2048]{0:T(1024)}, u32[]{:S(2)}) copy-start(f32[2048]{0:T(1024)} %param.30) | copy-start | bytes 24580
  144.1 42.9 %all-to-all-start.1 = ((bf16[8,16,256]{2,1,0:T(8,128)(2,1)}), bf16[8,16,256]{2,1,0:T(8,128)(2,1)S(1)}, u32[]{:S(2)}, u32[]{:S(2)}) async-start(bf16[8,16,256]{2,1,0:T(8,128)(2,1)} %bitcast.12), calls=%async_computation.1 | async-start | bytes 131072 | tf_op jit(solution)/shard_map/all_to_all | solution.py:141
  149.6 54.7 %all-reduce.5.cloned.1.call-start = ((), (), s32[]{:S(2)}) async-start(), calls=%async_computation.4 | async-start | bytes 131072 | tf_op jit(solution)/shard_map/psum | solution.py:142
  187.7 128.5 %reduce-scatter.2.cloned.1.call-start = ((), (), s32[]{:S(2)}) async-start(), calls=%async_computation.5 | async-start | bytes 1114112 | tf_op jit(solution)/shard_map/reduce_scatter | solution.py:165
  237.9 5.3 %copy-start.2 = (bf16[2048,352]{0,1:T(8,128)(2,1)S(1)}, bf16[2048,352]{0,1:T(8,128)(2,1)}, u32[]{:S(2)}) copy-start(bf16[2048,352]{0,1:T(8,128)(2,1)} %param.46) | copy-start | bytes 4325380
  244.7 9.1 %copy-start.3 = (bf16[2048,352]{0,1:T(8,128)(2,1)S(1)}, bf16[2048,352]{0,1:T(8,128)(2,1)}, u32[]{:S(2)}) copy-start(bf16[2048,352]{0,1:T(8,128)(2,1)} %param.47) | copy-start | bytes 4325380
Sparse Core Ops, SparseCore 0:
  59.3 16.3 all-reduce.2
  187.8 16.3 all-reduce.4
  257.7 58.4 reduce-scatter.1
where the time goes:
time: 325 us; the launch traced here: 324 us
  blocking collectives  133 us (41%)
  waiting for transfers between devices  97.7 us (30%)
  matrix products  46 us (14%)
  other arithmetic  15.8 us (5%)
  between operations  14.1 us (4%)
  starting transfers between devices  11.1 us (3%)
  local copies, waits for them, and re-layouts  6.74 us (2%)
    reduce_scatter x1, waiting for transfers between devices, body(): lax.psum_scatter(expert_term + branch_scale[:, None] * jnp.dot(shared_hid...  58.6 us
    all_gather x1, blocking collectives, body(): lax.all_gather(normed_half, 'ep', axis=0, tiled=True)  32.6 us
    all_gather x1, blocking collectives, body(): lax.all_gather(ffn_in, 'ep', axis=0, tiled=True)  31.8 us
    all_gather x1, blocking collectives, body(): lax.all_gather(attended, 'ep', axis=0, tiled=True)  31.1 us
    all_gather x1, blocking collectives, body(): lax.all_gather(chosen_coefficient, 'ep', axis=0, tiled=True)  20.9 us
    all_gather x1, blocking collectives, body(): lax.all_gather(chosen_specialist, 'ep', axis=0, tiled=True)  16.5 us
    psum x1, waiting for transfers between devices, body(): mixed_out = lax.psum(widen(out_part).astype(jnp.bfloat16), 'tp')  16.4 us
    psum x1, waiting for transfers between devices, body(): projected = lax.psum(widen(partial_value).astype(jnp.bfloat16), 'tp')  15.9 us
  transfers between devices with their start and end apart: 5, of which 4 were waited for; matrix products, arithmetic and copies ran while one was open for 1% of the time, Pallas kernels for 0%

commit v1 on v0

--- a/solution.py
+++ b/solution.py
@@ -1,6 +1,11 @@
+import functools
+import math
+
 import jax
 import jax.numpy as jnp
 from jax import lax
+from jax.experimental import pallas as pl
+from jax.experimental.pallas import tpu as pltpu
 from jax.sharding import PartitionSpec as P
 
 LANE_WIDTH = 64
@@ -10,6 +15,8 @@
 RMS_EPS = 1e-06
 GROUP_EPS = 0.00064
 HIGHEST = lax.Precision.HIGHEST
+MESH = pl.DeviceIdType.MESH
+VMEM_ROOM = 40 * 2**20
 
 
 def rms_norm(values, norm_gain):
@@ -174,6 +181,442 @@
     return ((own_residual + routed).astype(jnp.bfloat16), memory_after)
 
 
+def _others(ep, tp, fn):
+    me, core = lax.axis_index("ep"), lax.axis_index("tp")
+    for far in range(ep):
+        for side in range(tp):
+            if far or side:
+                fn(lax.rem(me + far, ep), lax.rem(core + side, tp))
+
+
+def _meet(ep, tp):
+    barrier = pltpu.get_barrier_semaphore()
+    _others(
+        ep,
+        tp,
+        lambda e, t: pl.semaphore_signal(
+            barrier, inc=1, device_id={"ep": e, "tp": t}, device_id_type=MESH
+        ),
+    )
+    pl.semaphore_wait(barrier, ep * tp - 1)
+
+
+def _remote(src, dst, send, recv, e, t):
+    return pltpu.make_async_remote_copy(
+        src_ref=src,
+        dst_ref=dst,
+        send_sem=send,
+        recv_sem=recv,
+        device_id={"ep": e, "tp": t},
+        device_id_type=MESH,
+    )
+
+
+def project_kernel(
+    ep, tp, x, gain, wq, wk, wv, fnar, fwid, fbias, lnar, lwid, lbias,
+    qkv, decay, rate,
+    halves, rows_all, w, part, got, wsem, ssem, rsem, psem, gsem, lsem,
+):
+    me, core = lax.axis_index("ep"), lax.axis_index("tp")
+    group = ep // tp
+    loads = [pltpu.make_async_copy(ref, w.at[i], wsem.at[i]) for i, ref in enumerate((wq, wk, wv))]
+    for load in loads:
+        load.start()
+    own, width = x.shape
+    half = width // tp
+    values = x[...].astype(jnp.float32)
+    normed = (rms_norm(values, gain[...])).astype(jnp.bfloat16)
+    for i in range(tp):
+        halves[i] = normed[:, i * half : (i + 1) * half]
+    _meet(ep, tp)
+    sends = []
+    for far in range(1, ep):
+        e = lax.rem(me + far, ep)
+        sends.append(
+            _remote(halves.at[core], rows_all.at[me], ssem.at[far], rsem.at[me], e, core)
+        )
+        sends[-1].start()
+    rows_all[me] = halves[core]
+    decay_mid = jnp.tanh(
+        jnp.dot(normed, fnar[...], preferred_element_type=jnp.float32)
+    ).astype(jnp.bfloat16)
+    decay_pre = fbias[...] + jnp.dot(decay_mid, fwid[...], preferred_element_type=jnp.float32)
+    decay[...] = jnp.exp(-(math.exp(-0.5) / (1.0 + jnp.exp(-decay_pre))))
+    rate_mid = jnp.dot(normed, lnar[...], preferred_element_type=jnp.float32).astype(jnp.bfloat16)
+    rate_pre = lbias[...] + jnp.dot(rate_mid, lwid[...], preferred_element_type=jnp.float32)
+    rate[...] = 1.0 / (1.0 + jnp.exp(-rate_pre))
+    for load in loads:
+        load.wait()
+    for far in range(1, ep):
+        e = lax.rem(me + far, ep)
+        pltpu.make_async_copy(rows_all.at[e], rows_all.at[e], rsem.at[e]).wait()
+    every = rows_all[...].reshape(ep * own, half)
+    for i in range(3):
+        done = jnp.dot(every, w[i], preferred_element_type=jnp.float32)
+        part[:, i] = done.astype(jnp.bfloat16).reshape(ep, own, done.shape[1])
+    goal = me // group
+    slot = core * group + lax.rem(me, group)
+    for far in range(1, ep):
+        e = lax.rem(me + far, ep)
+        _remote(part.at[e], got.at[slot], psem.at[far], gsem.at[slot], e, goal).start()
+    here = goal == core
+    local = pltpu.make_async_copy(part.at[me], got.at[slot], gsem.at[slot])
+    across = _remote(part.at[me], got.at[slot], psem.at[0], gsem.at[slot], me, goal)
+
+    @pl.when(here)
+    def _():
+        local.start()
+
+    @pl.when(jnp.logical_not(here))
+    def _():
+        across.start()
+
+    for i in range(ep):
+        pltpu.make_async_copy(got.at[i], got.at[i], gsem.at[i]).wait()
+    cols = w.shape[2]
+    for j in range(group):
+        for i in range(3):
+            total = got[j, i].astype(jnp.float32)
+            for s in range(1, tp):
+                total = total + got[s * group + j, i].astype(jnp.float32)
+            qkv[i, :, j * cols : (j + 1) * cols] = total.astype(jnp.bfloat16)
+    for send in sends:
+        send.wait_send()
+    for far in range(1, ep):
+        _remote(part.at[me], got.at[slot], psem.at[far], gsem.at[slot], me, goal).wait_send()
+
+    @pl.when(jnp.logical_not(here))
+    def _():
+        across.wait_send()
+
+
+def ffn_kernel(
+    ep, tp, expert_cols, att, x, ids, coef, gain, cs, wo_h, wg_h, wu_h, wd_h, cg_h, cu_h, cd_h,
+    out,
+    att_all, xcol, share, wo, wg, wu, wd, cg, cu, cd, pbuf, psib, res, ffn, hid, chid,
+    sibout, sibin, mine, got,
+    wsem, s_att, r_att, s_x, r_x, s_sh, r_sh, s_p, r_p, s_res, r_res, f_res, b_res,
+    s_sib, r_sib, s_out, r_out,
+):
+    me, core = lax.axis_index("ep"), lax.axis_index("tp")
+    mate = lax.rem(core + 1, tp)
+    group = ep // tp
+    own, width = x.shape
+    cols = wo.shape[1]
+    loads = [
+        pltpu.make_async_copy(a, b, wsem.at[i])
+        for i, (a, b) in enumerate(
+            ((wo_h, wo), (wg_h, wg), (wu_h, wu), (cg_h, cg), (cu_h, cu), (wd_h, wd), (cd_h, cd))
+        )
+    ]
+    for load in loads:
+        load.start()
+    lane = lax.broadcasted_iota(jnp.int32, (own, 128), 1)
+    routes = jnp.zeros((own, 128), jnp.float32)
+    for k in range(ids.shape[1]):
+        routes = routes + jnp.where(
+            ids[:, k : k + 1] == lane, coef[:, k : k + 1].astype(jnp.float32), 0.0
+        )
+    share[me] = routes
+    _meet(ep, tp)
+    sends = []
+
+    def push(*args):
+        sends.append(_remote(*args))
+        sends[-1].start()
+
+    for far in range(1, ep):
+        e = lax.rem(me + far, ep)
+        push(att, att_all.at[me], s_att.at[far], r_att.at[me], e, core)
+    for far in range(1, ep):
+        e = lax.rem(me + far, ep)
+        block = x.at[:, pl.ds(pl.multiple_of(e * cols, cols), cols)]
+        push(block, xcol.at[me], s_x.at[far], r_x.at[me], e, core)
+        push(share.at[me], share.at[me], s_sh.at[far], r_sh.at[me], e, core)
+    att_all[me] = att[...]
+    xcol[me] = x[:, pl.ds(pl.multiple_of(me * cols, cols), cols)]
+    loads[0].wait()
+
+    def arrive(ref, sem):
+        pltpu.make_async_copy(ref, ref, sem).wait()
+
+    for far in range(1, ep):
+        e = lax.rem(me + far, ep)
+        arrive(att_all.at[e], r_att.at[e])
+    half = att.shape[1]
+    done = jnp.dot(
+        att_all[...].reshape(ep * own, half), wo[...], preferred_element_type=jnp.float32
+    ).astype(jnp.bfloat16)
+    pbuf[...] = done.reshape(tp, group * own, cols)
+    push(pbuf.at[mate], psib, s_p, r_p, me, mate)
+    for far in range(1, ep):
+        e = lax.rem(me + far, ep)
+        arrive(xcol.at[e], r_x.at[e])
+    arrive(psib, r_p)
+    mixed = (pbuf[core].astype(jnp.float32) + psib[...].astype(jnp.float32)).astype(jnp.bfloat16)
+    held = xcol[pl.ds(core * group, group)].reshape(group * own, cols).astype(jnp.float32)
+    res[me, core] = (held + mixed.astype(jnp.float32)).astype(jnp.bfloat16)
+    for far in range(1, ep):
+        e = lax.rem(me + far, ep)
+        push(res.at[me, core], res.at[me, core], s_res.at[far], r_res.at[me], e, core)
+    push(res.at[me, core], res.at[me, core], f_res.at[me], b_res.at[me], me, mate)
+    for far in range(1, ep):
+        e = lax.rem(me + far, ep)
+        arrive(res.at[e, core], r_res.at[e])
+        push(res.at[e, core], res.at[e, core], f_res.at[e], b_res.at[e], me, mate)
+    for far in range(ep):
+        e = lax.rem(me + far, ep)
+        arrive(res.at[e, mate], b_res.at[e])
+    rows = ep * own
+    square = jnp.zeros((rows, 1), jnp.float32)
+    for s in range(ep):
+        block = res[s].reshape(rows, cols).astype(jnp.float32)
+        square = square + jnp.sum(block * block, axis=-1, keepdims=True)
+    inv = lax.rsqrt(square / width + RMS_EPS)
+    gate_sum = jnp.zeros((rows, 1), jnp.float32)
+    for s in range(ep):
+        at = slice(s * cols, (s + 1) * cols)
+        block = res[s].reshape(rows, cols).astype(jnp.float32)
+        block = (block * inv * gain[:, at]).astype(jnp.bfloat16)
+        ffn[:, at] = block
+        gate_sum = gate_sum + jnp.sum(
+            block.astype(jnp.float32) * cs[:, at].astype(jnp.float32), axis=-1, keepdims=True
+        )
+    branch_scale = 1.0 / (1.0 + jnp.exp(-gate_sum))
+    for far in range(1, ep):
+        e = lax.rem(me + far, ep)
+        arrive(share.at[e], r_sh.at[e])
+    expert = (me * tp + core) * wg.shape[1] // expert_cols
+    table = share[...].reshape(rows, 128)
+    picked = lax.broadcasted_iota(jnp.int32, (rows, 128), 1) == expert
+    weight = jnp.sum(jnp.where(picked, table, 0.0), axis=-1, keepdims=True)
+    for i in (1, 2):
+        loads[i].wait()
+
+    def widen_up(c, _):
+        at = pl.ds(pl.multiple_of(c * 256, 256), 256)
+        g = jnp.dot(ffn[...], wg[:, at], preferred_element_type=jnp.float32)
+        u = jnp.dot(ffn[...], wu[:, at], preferred_element_type=jnp.float32)
+        hid[:, at] = (g / (1.0 + jnp.exp(-g)) * u).astype(jnp.bfloat16)
+        return _
+
+    lax.fori_loop(0, wg.shape[1] // 256, widen_up, 0)
+    for i in (3, 4):
+        loads[i].wait()
+    g = jnp.dot(ffn[...], cg[...], preferred_element_type=jnp.float32)
+    u = jnp.dot(ffn[...], cu[...], preferred_element_type=jnp.float32)
+    chid[...] = (g / (1.0 + jnp.exp(-g)) * u).astype(jnp.bfloat16)
+    for i in (5, 6):
+        loads[i].wait()
+    pieces = mine.shape[0]
+    piece = width // pieces
+    last = own // tp
+    for n in range(pieces):
+        at = slice(n * piece, (n + 1) * piece)
+        y = weight * jnp.dot(hid[...], wd[:, at], preferred_element_type=jnp.float32)
+        y = y + branch_scale * jnp.dot(chid[...], cd[:, at], preferred_element_type=jnp.float32)
+        y = y.reshape(ep, tp, last, piece)
+        for side in range(tp):
+            sibout[n, side] = y[:, side].astype(jnp.bfloat16)
+        push(sibout.at[n, mate], sibin.at[n], s_sib.at[n], r_sib.at[n], me, mate)
+    for n in range(pieces):
+        arrive(sibin.at[n], r_sib.at[n])
+        mine[n] = (
+            sibout[n, core].astype(jnp.float32) + sibin[n].astype(jnp.float32)
+        ).astype(jnp.bfloat16)
+        for far in range(1, ep):
+            e = lax.rem(me + far, ep)
+            push(mine.at[n, e], got.at[n, me], s_out.at[n, far], r_out.at[n, me], e, core)
+    start = pl.multiple_of(lax.rem(me, group) * own, own)
+    per = piece // cols
+    for n in range(pieces):
+        total = mine[n, me].astype(jnp.float32)
+        for far in range(1, ep):
+            e = lax.rem(me + far, ep)
+            arrive(got.at[n, e], r_out.at[n, e])
+            total = total + got[n, e].astype(jnp.float32)
+        for s in range(per):
+            base = res[n * per + s, me // group, pl.ds(start, own)].astype(jnp.float32)
+            base = jnp.where(core == 0, base[:last], base[last:])
+            a = n * piece + s * cols
+            out[:, a : a + cols] = (base + total[:, s * cols : (s + 1) * cols]).astype(jnp.bfloat16)
+    for send in sends:
+        send.wait_send()
+
+
+def layer(*blocks):
+    own = blocks[0].shape[0]
+    cols, hidden = blocks[9].shape[1], blocks[18].shape[1]
+    tiles = cols % 128 == 0 and hidden % 256 == 0 and own % 16 == 0
+    heads_match = lax.axis_size("ep") % lax.axis_size("tp") == 0 and lax.axis_size("tp") == 2
+    weights = sum(2 * w.size for w in blocks[18:24])
+    rows = own * lax.axis_size("ep")
+    held = weights + rows * (12 * blocks[0].shape[1] + 8 * hidden)
+    small = held < VMEM_ROOM
+    return (kernel_body if tiles and heads_match and small else body)(*blocks)
+
+
+def kernel_body(
+    fresh_inputs,
+    memory_arrays,
+    chosen_specialist,
+    chosen_coefficient,
+    first_rescale,
+    second_rescale,
+    receiver_projector,
+    address_projector,
+    content_projector,
+    final_projector,
+    forget_narrowing,
+    forget_widening,
+    forget_bias,
+    learning_narrowing,
+    learning_widening,
+    learning_bias,
+    lane_scaling,
+    instant_reward,
+    specialist_switch,
+    specialist_expand,
+    specialist_contract,
+    common_activator,
+    common_expand,
+    common_contract,
+    common_switch,
+):
+    ep, tp = lax.axis_size("ep"), lax.axis_size("tp")
+    own, width = fresh_inputs.shape
+    half, cols = width // tp, final_projector.shape[1]
+    heads = half // LANE_WIDTH
+    group = ep // tp
+    vmem = pl.BlockSpec(memory_space=pltpu.VMEM)
+    hbm = pl.BlockSpec(memory_space=pl.ANY)
+    bf16, f32 = jnp.bfloat16, jnp.float32
+    dma = pltpu.SemaphoreType.DMA
+
+    def row(vector):
+        return vector.reshape(1, -1)
+
+    qkv, decay_vals, rate_vals = pl.pallas_call(
+        functools.partial(project_kernel, ep, tp),
+        out_shape=(
+            jax.ShapeDtypeStruct((3, own, half), bf16),
+            jax.ShapeDtypeStruct((own, half), f32),
+            jax.ShapeDtypeStruct((own, half), f32),
+        ),
+        in_specs=[vmem] * 2 + [hbm] * 3 + [vmem] * 6,
+        out_specs=(vmem,) * 3,
+        scratch_shapes=[
+            pltpu.VMEM((tp, own, half), bf16),
+            pltpu.VMEM((ep, own, half), bf16),
+            pltpu.VMEM((3, half, cols), bf16),
+            pltpu.VMEM((ep, 3, own, cols), bf16),
+            pltpu.VMEM((ep, 3, own, cols), bf16),
+            dma((3,)),
+            dma((ep,)),
+            dma((ep,)),
+            dma((ep,)),
+            dma((ep,)),
+            dma((1,)),
+        ],
+        compiler_params=pltpu.CompilerParams(collective_id=0, has_side_effects=True),
+        name="project",
+    )(
+        fresh_inputs,
+        row(first_rescale),
+        receiver_projector,
+        address_projector,
+        content_projector,
+        forget_narrowing,
+        forget_widening,
+        row(forget_bias),
+        learning_narrowing,
+        learning_widening,
+        row(learning_bias),
+    )
+
+    def divide_lanes(channels):
+        return channels.astype(jnp.float32).reshape(own, heads, LANE_WIDTH)
+
+    memory_after, memory_retrieval = evolve_memory(
+        memory_arrays,
+        divide_lanes(qkv[0]),
+        divide_lanes(qkv[1]),
+        divide_lanes(qkv[2]),
+        divide_lanes(decay_vals),
+        divide_lanes(rate_vals),
+        lane_scaling.reshape(heads, LANE_WIDTH),
+        instant_reward,
+    )
+    attended = memory_retrieval.reshape(own, half).astype(jnp.bfloat16)
+    rows, hidden, dense = ep * own, specialist_switch.shape[1], common_activator.shape[1]
+    pieces = 4
+    piece, last = width // pieces, own // tp
+    new_tokens = pl.pallas_call(
+        functools.partial(ffn_kernel, ep, tp, FF_E),
+        out_shape=jax.ShapeDtypeStruct((last, width), bf16),
+        in_specs=[vmem] * 6 + [hbm] * 7,
+        out_specs=vmem,
+        scratch_shapes=[
+            pltpu.VMEM((ep, own, half), bf16),
+            pltpu.VMEM((ep, own, cols), bf16),
+            pltpu.VMEM((ep, own, 128), f32),
+            pltpu.VMEM((half, cols), bf16),
+            pltpu.VMEM((width, hidden), bf16),
+            pltpu.VMEM((width, hidden), bf16),
+            pltpu.VMEM((hidden, width), bf16),
+            pltpu.VMEM((width, dense), bf16),
+            pltpu.VMEM((width, dense), bf16),
+            pltpu.VMEM((dense, width), bf16),
+            pltpu.VMEM((tp, group * own, cols), bf16),
+            pltpu.VMEM((group * own, cols), bf16),
+            pltpu.VMEM((ep, tp, group * own, cols), bf16),
+            pltpu.VMEM((rows, width), bf16),
+            pltpu.VMEM((rows, hidden), bf16),
+            pltpu.VMEM((rows, dense), bf16),
+            pltpu.VMEM((pieces, tp, ep, last, piece), bf16),
+            pltpu.VMEM((pieces, ep, last, piece), bf16),
+            pltpu.VMEM((pieces, ep, last, piece), bf16),
+            pltpu.VMEM((pieces, ep, last, piece), bf16),
+            dma((7,)),
+            dma((ep,)),
+            dma((ep,)),
+            dma((ep,)),
+            dma((ep,)),
+            dma((ep,)),
+            dma((ep,)),
+            dma,
+            dma,
+            dma((ep,)),
+            dma((ep,)),
+            dma((ep,)),
+            dma((ep,)),
+            dma((pieces,)),
+            dma((pieces,)),
+            dma((pieces, ep)),
+            dma((pieces, ep)),
+        ],
+        compiler_params=pltpu.CompilerParams(
+            collective_id=1, has_side_effects=True, vmem_limit_bytes=56 * 2**20
+        ),
+        name="experts",
+    )(
+        attended,
+        fresh_inputs,
+        chosen_specialist,
+        chosen_coefficient,
+        row(second_rescale),
+        row(common_switch),
+        final_projector,
+        specialist_switch,
+        specialist_expand,
+        specialist_contract,
+        common_activator,
+        common_expand,
+        common_contract,
+    )
+    return (new_tokens, memory_after)
+
+
 def solution(mesh):
     placed = (
         P(("grp", "ep"), None),
@@ -203,7 +646,7 @@
         P(),
     )
     return jax.shard_map(
-        body,
+        layer,
         mesh=mesh,
         in_specs=placed,
         out_specs=(P(("grp", "ep", "tp"), None), P(("grp", "ep"), "tp", None, None)),

time: 325 us -> 113 us (0.35)
  blocking collectives: 133 us -> 0 us
  waiting for transfers between devices: 97.7 us -> 0 us
  Pallas kernels: 0 us -> 62.1 us
  matrix products: 46 us -> 24.5 us
  between operations: 14.1 us -> 0.77 us
  starting transfers between devices: 11.1 us -> 0 us
  local copies, waits for them, and re-layouts: 6.74 us -> 12.7 us
  other arithmetic: 15.8 us -> 12.5 us
    all_gather x5 -> x0, blocking collectives: 133 us -> none  [the longest x1 32.6 us: body(): lax.all_gather(normed_half, 'ep', axis=0, tiled=True)]
    pallas_call x0 -> x2, Pallas kernels: none -> 62.1 us  [the longest x1 41.8 us: kernel_body(): pl.pallas_call(functools.partial(ffn_kernel, ep, tp, FF_E), out_shape=jax...]
    reduce_scatter x1 -> x0, waiting for transfers between devices: 58.6 us -> none  [body(): lax.psum_scatter(expert_term + branch_scale[:, None] * jnp.dot(shared_hid...]
    psum x2 -> x0, waiting for transfers between devices: 32.3 us -> none  [the longest x1 16.4 us: body(): mixed_out = lax.psum(widen(out_part).astype(jnp.bfloat16), 'tp')]
    dot_general x9 -> x0, matrix products: 23.9 us -> none  [the longest x1 9.06 us: body(): jnp.dot(hidden, specialist_contract, preferred_element_type=jnp.float32)]
    all_to_all x2 -> x0, starting transfers between devices: 11 us -> none  [the longest x1 5.52 us: body(): lax.all_to_all(projected_rows, 'ep', split_axis=0, concat_axis=2, tiled=T...]
    all_to_all x2 -> x0, waiting for transfers between devices: 6.71 us -> none  [the longest x1 6.7 us: body(): lax.all_to_all(projected_rows, 'ep', split_axis=0, concat_axis=2, tiled=T...]
    unnamed x31 -> x23, local copies, waits for them, and re-layouts: 3.47 us -> 9.83 us
  transfers between devices with their start and end apart: 5 -> 0, of which waited for: 4 -> 0; matrix products, arithmetic and copies ran while one was open for 1% -> 0% of each run, Pallas kernels for 0% -> 0%
where the time goes in v1:
time: 113 us; the launch traced here: 112 us
  Pallas kernels  62.1 us (55%)
  matrix products  24.5 us (22%)
  local copies, waits for them, and re-layouts  12.7 us (11%)
  other arithmetic  12.5 us (11%)
    pallas_call x1, Pallas kernels, kernel_body(): pl.pallas_call(functools.partial(ffn_kernel, ep, tp, FF_E), out_shape=jax...  41.8 us
    pallas_call x1, Pallas kernels, kernel_body(): pl.pallas_call(functools.partial(project_kernel, ep, tp), out_shape=(jax....  20.3 us
    dot_general x1, matrix products, evolve_memory(): jnp.einsum('bhvk,bhk->bhv', memory_arrays, unit_key, precision=HIGHEST)  15.4 us
    add x1, other arithmetic, evolve_memory(): memory_arrays * forget_lanes[:, :, None, :]  10.6 us
    unnamed x23, local copies, waits for them, and re-layouts  9.83 us
    dot_general x1, matrix products, evolve_memory(): jnp.einsum('bhvk,bhk->bhv', memory_after, receiver_lanes, precision=HIGHEST)  9.07 us

profile of v1, /device:TPU:0, one launch (start us, length us, event | category | flops | bytes accessed | tf_op | source)
XLA Modules:
  0.0 112.5 jit_solution(6219360590586278176)
XLA Ops:
  0.6 2.0 %copy.27.fnar = bf16[2048,64]{1,0:T(8,128)(2,1)} copy(bf16[2048,64]{0,1:T(8,128)(2,1)} %param.35) | data formatting | bytes 524288 | tf_op args[10]
  2.6 1.9 %copy.28.lnar = bf16[2048,64]{1,0:T(8,128)(2,1)} copy(bf16[2048,64]{0,1:T(8,128)(2,1)} %param.38) | data formatting | bytes 524288 | tf_op args[13]
  4.5 20.3 %project.1 = (bf16[3,16,1024]{2,1,0:T(8,128)(2,1)}, f32[16,1024]{1,0:T(8,128)}, f32[16,1024]{1,0:T(8,128)}) custom-call(bf16[16,2048]{1,0:T(8,128)(2,1)} %x.3, f32[1,2048]{1,0:T(1,128)} %bitcast.20, bf16[1024,256]{1,0:T(8,128)(2,1)} %wq.1, bf16[1024,256]{1,0:T(8,128)(2,1)} %wk.1, bf16[1024,256]{1,0:T(8,128)(2,1)} %wv.1, bf16[2048,64]{1,0:T(8,128)(2,1)} %copy.27.fnar, ...), custom_call_target="tpu_custom_call" | custom-call | tf_op jit(solution)/shard_map/project/pallas_call | solution.py:499
  24.8 0.0 copy-start.2
  24.9 0.8 fusion.7
  25.7 0.1 reshape.99
  25.8 0.1 multiply_reduce_fusion.1
  25.9 0.9 reshape.95
  26.8 0.1 fusion.6
  26.9 15.4 %fusion.8 = f32[16,16,1,64]{3,2,1,0:T(1,128)S(1)} fusion(f32[16,16,64,1]{2,3,1,0:T(1,128)S(1)} %bitcast.19, f32[16,16,64,64]{3,2,1,0:T(8,128)} %param.26), kind=kOutput, calls=%fused_computation.18 | convolution fusion | flops 12582912 | bytes 4325376 | tf_op jit(solution)/shard_map/bhvk,bhk->bhv/dot_general | solution.py:45
  42.3 0.1 reshape.100
  42.4 0.0 copy-done.2
  42.4 0.1 mul.121
  42.5 10.6 %multiply_add_fusion = f32[16,16,64,64]{3,2,1,0:T(8,128)} fusion(f32[16,16,64,64]{3,2,1,0:T(8,128)} %param.26, f32[16,16,64]{2,1,0:T(8,128)S(1)} %get-tuple-element.10, f32[16,16,64]{2,1,0:T(8,128)S(1)} %reshape.100, f32[16,16,64]{2,1,0:T(8,128)S(1)} %get-tuple-element.8, f32[16,16,64]{2,1,0:T(8,128)S(1)} %bitcast.18, f32[16,16,64]{2,1,0:T(8,128)S(1)} %mul.121), kind=kLoop, calls=%fused_computation.1 | loop fusion | flops 5242880 | bytes 8716288 | tf_op jit(solution)/shard_map/add | solution.py:47
  53.1 0.0 copy-start.4
  53.1 0.0 copy-start.3
  53.1 0.0 copy-start
  53.1 0.0 copy-start.1
  53.1 0.0 copy-start.6
  53.1 0.0 copy-start.5
  53.1 0.0 copy-start.7
  53.2 0.1 reshape.106
  53.3 9.1 %fusion.9 = f32[16,16,1,64]{3,2,1,0:T(1,128)S(1)} fusion(f32[16,16,64,64]{3,2,1,0:T(8,128)} %multiply_add_fusion, bf16[16,16,64,1]{2,3,1,0:T(2,128)(2,1)S(1)} %reshape.106), kind=kOutput, calls=%fused_computation.19 | convolution fusion | flops 12582912 | bytes 4292608 | tf_op jit(solution)/shard_map/bhvk,bhk->bhv/dot_general | solution.py:51
  62.4 0.1 reduce_sum.37
  62.5 0.2 multiply_reduce_fusion
  62.7 0.1 reshape.96
  62.8 0.0 copy-done.4
  62.8 0.1 mul.138
  62.9 0.0 copy-done.3
  62.9 0.5 fusion.3
  63.4 0.7 convert_element_type.52.att
  64.2 0.0 copy-done
  64.2 1.6 %copy.31.cg_h = bf16[2048,352]{1,0:T(8,128)(2,1)} copy(bf16[2048,352]{0,1:T(8,128)(2,1)S(1)} %copy-done) | data formatting | bytes 2883584 | tf_op args[21]
  65.7 0.0 copy-done.1
  65.7 1.6 %copy.32.cu_h = bf16[2048,352]{1,0:T(8,128)(2,1)} copy(bf16[2048,352]{0,1:T(8,128)(2,1)S(1)} %copy-done.1) | data formatting | bytes 2883584 | tf_op args[22]
  67.3 0.0 copy-done.6
  67.3 0.7 copy.29.ids
  68.0 0.0 copy-done.5
  68.0 0.6 reshape.98.cs
  68.6 0.0 copy-done.7
  68.6 0.7 copy.30.coef
  69.3 41.8 %experts.1 = bf16[8,2048]{1,0:T(8,128)(2,1)} custom-call(bf16[16,1024]{1,0:T(8,128)(2,1)} %convert_element_type.52.att, bf16[16,2048]{1,0:T(8,128)(2,1)} %x.3, s32[16,2]{1,0:T(8,128)} %copy.29.ids, bf16[16,2]{1,0:T(8,128)(2,1)} %copy.30.coef, f32[1,2048]{1,0:T(1,128)} %bitcast.21, bf16[1,2048]{1,0:T(2,128)(2,1)} %reshape.98.cs, bf16[1024,256]{1,0:T(8,128)(2,1)} %wo_h.1, ...), custom_call_target="tpu_custom_call" | custom-call | tf_op jit(solution)/shard_map/experts/pallas_call | solution.py:554
  111.1 1.4 %copy.38 = bf16[8,2048]{1,0:T(8,128)(2,1)} copy(bf16[8,2048]{1,0:T(8,128)(2,1)} %experts.1) | data formatting | bytes 65536
  (3 shorter events, 0.0 us)
Async XLA Ops:
  24.8 17.6 %copy-start.2 = (f32[16,1024]{1,0:T(8,128)S(1)}, f32[16,1024]{1,0:T(8,128)}, u32[]{:S(2)}) copy-start(f32[16,1024]{1,0:T(8,128)} %get-tuple-element.5) | copy-start | bytes 196612
  53.1 9.7 %copy-start.4 = (f32[1024]{0:T(1024)S(1)}, f32[1024]{0:T(1024)}, u32[]{:S(2)}) copy-start(f32[1024]{0:T(1024)} %param.41) | copy-start | bytes 12292
  53.1 9.8 %copy-start.3 = (f32[16,64]{1,0:T(8,128)S(1)}, f32[16,64]{1,0:T(8,128)}, u32[]{:S(2)}) copy-start(f32[16,64]{1,0:T(8,128)} %param.42) | copy-start | bytes 12292
  53.1 11.0 %copy-start = (bf16[2048,352]{0,1:T(8,128)(2,1)S(1)}, bf16[2048,352]{0,1:T(8,128)(2,1)}, u32[]{:S(2)}) copy-start(bf16[2048,352]{0,1:T(8,128)(2,1)} %param.46) | copy-start | bytes 4325380
  53.1 12.6 %copy-start.1 = (bf16[2048,352]{0,1:T(8,128)(2,1)S(1)}, bf16[2048,352]{0,1:T(8,128)(2,1)}, u32[]{:S(2)}) copy-start(bf16[2048,352]{0,1:T(8,128)(2,1)} %param.47) | copy-start | bytes 4325380
  53.1 14.2 %copy-start.6 = (s32[16,2]{0,1:T(2,128)S(1)}, s32[16,2]{0,1:T(2,128)}, u32[]{:S(2)}) copy-start(s32[16,2]{0,1:T(2,128)} %param.27) | copy-start | bytes 388
  53.1 14.9 %copy-start.5 = (bf16[2048]{0:T(1024)(128)(2,1)S(1)}, bf16[2048]{0:T(1024)(128)(2,1)}, u32[]{:S(2)}) copy-start(bf16[2048]{0:T(1024)(128)(2,1)} %param.49) | copy-start | bytes 12292
  53.1 15.5 %copy-start.7 = (bf16[16,2]{0,1:T(2,128)(2,1)S(1)}, bf16[16,2]{0,1:T(2,128)(2,1)}, u32[]{:S(2)}) copy-start(bf16[16,2]{0,1:T(2,128)(2,1)} %param.28) | copy-start | bytes 196

commit v2 on v1

--- a/solution.py
+++ b/solution.py
@@ -212,9 +212,55 @@
     )
 
 
+def across_dot(left, right):
+    return lax.dot_general(
+        left, right, (((1,), (1,)), ((), ())), preferred_element_type=jnp.float32
+    )
+
+
+def by_head(ref, channels, first):
+    for h in range(channels.shape[1] // LANE_WIDTH):
+        ref[:, first + h, :] = channels[:, h * LANE_WIDTH : (h + 1) * LANE_WIDTH]
+
+
+def state_kernel(memory, query, key, value, decay, rate, lane_gain, reward, after, read, flip):
+    count, heads = query.shape[0], query.shape[1]
+    lane = lax.broadcasted_iota(jnp.int32, (LANE_WIDTH, 128), 1)
+
+    def sequence(b, carry):
+        q, k, v, d, r = query[b], key[b], value[b], decay[b], rate[b]
+        unit = k * lax.rsqrt(jnp.sum(k * k, axis=-1, keepdims=True) + 1.0)
+        scaled, pulled, seen = k * r, unit * r, d * q
+        flip[0:heads] = v
+        value_cols = flip[...].T
+        found = jnp.zeros((LANE_WIDTH, 128), jnp.float32)
+        for h in range(heads):
+            one = slice(h, h + 1)
+            m = memory[b, h]
+            removal = jnp.sum(m * unit[one], axis=-1, keepdims=True)
+            kept = jnp.sum(m * seen[one], axis=-1, keepdims=True)
+            after[b, h] = m * d[one] - removal * pulled[one] + value_cols[:, one] * scaled[one]
+            found = jnp.where(lane == h, removal, found)
+            found = jnp.where(lane == heads + h, kept, found)
+        rows = found.T
+        out = (
+            rows[heads : 2 * heads]
+            - rows[0:heads] * jnp.sum(pulled * q, axis=-1, keepdims=True)
+            + v * jnp.sum(scaled * q, axis=-1, keepdims=True)
+        )
+        centred = out - jnp.mean(out, axis=-1, keepdims=True)
+        level = lax.rsqrt(jnp.mean(centred * centred, axis=-1, keepdims=True) + GROUP_EPS)
+        extra = jnp.sum(q * scaled * reward[...], axis=-1, keepdims=True) * v
+        read[b] = centred * level * lane_gain[...] + extra
+        return carry
+
+    flip[...] = jnp.zeros_like(flip)
+    lax.fori_loop(0, count, sequence, 0)
+
+
 def project_kernel(
-    ep, tp, x, gain, wq, wk, wv, fnar, fwid, fbias, lnar, lwid, lbias,
-    qkv, decay, rate,
+    ep, tp, x, gain, wq, wk, wv, fnar, fwid, fbias, lnar, lwid, lbias, scaling,
+    query, key, value, decay, rate, lane_gain,
     halves, rows_all, w, part, got, wsem, ssem, rsem, psem, gsem, lsem,
 ):
     me, core = lax.axis_index("ep"), lax.axis_index("tp")
@@ -237,14 +283,14 @@
         )
         sends[-1].start()
     rows_all[me] = halves[core]
-    decay_mid = jnp.tanh(
-        jnp.dot(normed, fnar[...], preferred_element_type=jnp.float32)
-    ).astype(jnp.bfloat16)
+    decay_mid = jnp.tanh(across_dot(normed, fnar[...])).astype(jnp.bfloat16)
     decay_pre = fbias[...] + jnp.dot(decay_mid, fwid[...], preferred_element_type=jnp.float32)
-    decay[...] = jnp.exp(-(math.exp(-0.5) / (1.0 + jnp.exp(-decay_pre))))
-    rate_mid = jnp.dot(normed, lnar[...], preferred_element_type=jnp.float32).astype(jnp.bfloat16)
+    by_head(decay, jnp.exp(-(math.exp(-0.5) / (1.0 + jnp.exp(-decay_pre)))), 0)
+    rate_mid = across_dot(normed, lnar[...]).astype(jnp.bfloat16)
     rate_pre = lbias[...] + jnp.dot(rate_mid, lwid[...], preferred_element_type=jnp.float32)
-    rate[...] = 1.0 / (1.0 + jnp.exp(-rate_pre))
+    by_head(rate, 1.0 / (1.0 + jnp.exp(-rate_pre)), 0)
+    for h in range(lane_gain.shape[0]):
+        lane_gain[h : h + 1] = scaling[:, h * LANE_WIDTH : (h + 1) * LANE_WIDTH]
     for load in loads:
         load.wait()
     for far in range(1, ep):
@@ -279,7 +325,8 @@
             total = got[j, i].astype(jnp.float32)
             for s in range(1, tp):
                 total = total + got[s * group + j, i].astype(jnp.float32)
-            qkv[i, :, j * cols : (j + 1) * cols] = total.astype(jnp.bfloat16)
+            total = total.astype(jnp.bfloat16).astype(jnp.float32)
+            by_head((query, key, value)[i], total, j * (cols // LANE_WIDTH))
     for send in sends:
         send.wait_send()
     for far in range(1, ep):
@@ -291,9 +338,9 @@
 
 
 def ffn_kernel(
-    ep, tp, expert_cols, att, x, ids, coef, gain, cs, wo_h, wg_h, wu_h, wd_h, cg_h, cu_h, cd_h,
+    ep, tp, expert_cols, read, x, ids, coef, gain, cs, wo_h, wg_h, wu_h, wd_h, cg_h, cu_h, cd_h,
     out,
-    att_all, xcol, share, wo, wg, wu, wd, cg, cu, cd, pbuf, psib, res, ffn, hid, chid,
+    att, att_all, xcol, share, wo, wg, wu, wd, cg, cu, cd, pbuf, psib, res, ffn, hid, chid,
     sibout, sibin, mine, got,
     wsem, s_att, r_att, s_x, r_x, s_sh, r_sh, s_p, r_p, s_res, r_res, f_res, b_res,
     s_sib, r_sib, s_out, r_out,
@@ -313,11 +360,16 @@
         load.start()
     lane = lax.broadcasted_iota(jnp.int32, (own, 128), 1)
     routes = jnp.zeros((own, 128), jnp.float32)
-    for k in range(ids.shape[1]):
+    ids_cols, coef_cols = ids[...].T, coef[...].astype(jnp.float32).T
+    for k in range(ids.shape[0]):
         routes = routes + jnp.where(
-            ids[:, k : k + 1] == lane, coef[:, k : k + 1].astype(jnp.float32), 0.0
+            ids_cols[:, k : k + 1] == lane, coef_cols[:, k : k + 1], 0.0
         )
     share[me] = routes
+    pack = 128 // LANE_WIDTH
+    for h in range(0, read.shape[1], pack):
+        joined = jnp.concatenate([read[:, h + i, :] for i in range(pack)], axis=-1)
+        att[:, h * LANE_WIDTH : h * LANE_WIDTH + 128] = joined.astype(jnp.bfloat16)
     _meet(ep, tp)
     sends = []
 
@@ -403,8 +455,7 @@
     lax.fori_loop(0, wg.shape[1] // 256, widen_up, 0)
     for i in (3, 4):
         loads[i].wait()
-    g = jnp.dot(ffn[...], cg[...], preferred_element_type=jnp.float32)
-    u = jnp.dot(ffn[...], cu[...], preferred_element_type=jnp.float32)
+    g, u = across_dot(ffn[...], cg[...]), across_dot(ffn[...], cu[...])
     chid[...] = (g / (1.0 + jnp.exp(-g)) * u).astype(jnp.bfloat16)
     for i in (5, 6):
         loads[i].wait()
@@ -496,15 +547,12 @@
     def row(vector):
         return vector.reshape(1, -1)
 
-    qkv, decay_vals, rate_vals = pl.pallas_call(
+    per_head = jax.ShapeDtypeStruct((own, heads, LANE_WIDTH), f32)
+    *lanes, lane_gain = pl.pallas_call(
         functools.partial(project_kernel, ep, tp),
-        out_shape=(
-            jax.ShapeDtypeStruct((3, own, half), bf16),
-            jax.ShapeDtypeStruct((own, half), f32),
-            jax.ShapeDtypeStruct((own, half), f32),
-        ),
-        in_specs=[vmem] * 2 + [hbm] * 3 + [vmem] * 6,
-        out_specs=(vmem,) * 3,
+        out_shape=(per_head,) * 5 + (jax.ShapeDtypeStruct((heads, LANE_WIDTH), f32),),
+        in_specs=[vmem] * 2 + [hbm] * 3 + [vmem] * 7,
+        out_specs=(vmem,) * 6,
         scratch_shapes=[
             pltpu.VMEM((tp, own, half), bf16),
             pltpu.VMEM((ep, own, half), bf16),
@@ -526,28 +574,27 @@
         receiver_projector,
         address_projector,
         content_projector,
-        forget_narrowing,
+        forget_narrowing.T,
         forget_widening,
         row(forget_bias),
-        learning_narrowing,
+        learning_narrowing.T,
         learning_widening,
         row(learning_bias),
-    )
-
-    def divide_lanes(channels):
-        return channels.astype(jnp.float32).reshape(own, heads, LANE_WIDTH)
-
-    memory_after, memory_retrieval = evolve_memory(
-        memory_arrays,
-        divide_lanes(qkv[0]),
-        divide_lanes(qkv[1]),
-        divide_lanes(qkv[2]),
-        divide_lanes(decay_vals),
-        divide_lanes(rate_vals),
-        lane_scaling.reshape(heads, LANE_WIDTH),
-        instant_reward,
-    )
-    attended = memory_retrieval.reshape(own, half).astype(jnp.bfloat16)
+        row(lane_scaling),
+    )
+    step = 2
+    lane_spec = pl.BlockSpec((step, heads, LANE_WIDTH), lambda i: (i, 0, 0))
+    gain_spec = pl.BlockSpec((heads, LANE_WIDTH), lambda i: (0, 0))
+    memory_spec = pl.BlockSpec((step, heads, LANE_WIDTH, LANE_WIDTH), lambda i: (i, 0, 0, 0))
+    memory_after, read = pl.pallas_call(
+        state_kernel,
+        grid=(own // step,),
+        out_shape=(jax.ShapeDtypeStruct(memory_arrays.shape, f32), per_head),
+        in_specs=[memory_spec] + [lane_spec] * 5 + [gain_spec] * 2,
+        out_specs=(memory_spec, lane_spec),
+        scratch_shapes=[pltpu.VMEM((128, LANE_WIDTH), f32)],
+        name="state",
+    )(memory_arrays, *lanes, lane_gain, instant_reward)
     rows, hidden, dense = ep * own, specialist_switch.shape[1], common_activator.shape[1]
     pieces = 4
     piece, last = width // pieces, own // tp
@@ -557,6 +604,7 @@
         in_specs=[vmem] * 6 + [hbm] * 7,
         out_specs=vmem,
         scratch_shapes=[
+            pltpu.VMEM((own, half), bf16),
             pltpu.VMEM((ep, own, half), bf16),
             pltpu.VMEM((ep, own, cols), bf16),
             pltpu.VMEM((ep, own, 128), f32),
@@ -564,8 +612,8 @@
             pltpu.VMEM((width, hidden), bf16),
             pltpu.VMEM((width, hidden), bf16),
             pltpu.VMEM((hidden, width), bf16),
-            pltpu.VMEM((width, dense), bf16),
-            pltpu.VMEM((width, dense), bf16),
+            pltpu.VMEM((dense, width), bf16),
+            pltpu.VMEM((dense, width), bf16),
             pltpu.VMEM((dense, width), bf16),
             pltpu.VMEM((tp, group * own, cols), bf16),
             pltpu.VMEM((group * own, cols), bf16),
@@ -600,18 +648,18 @@
         ),
         name="experts",
     )(
-        attended,
+        read,
         fresh_inputs,
-        chosen_specialist,
-        chosen_coefficient,
+        chosen_specialist.T,
+        chosen_coefficient.T,
         row(second_rescale),
         row(common_switch),
         final_projector,
         specialist_switch,
         specialist_expand,
         specialist_contract,
-        common_activator,
-        common_expand,
+        common_activator.T,
+        common_expand.T,
         common_contract,
     )
     return (new_tokens, memory_after)

time: 113 us -> 88.1 us (0.78)
  matrix products: 24.5 us -> 0 us
  Pallas kernels: 62.1 us -> 85.2 us
  other arithmetic: 12.5 us -> 0 us
  local copies, waits for them, and re-layouts: 12.7 us -> 1.98 us
    dot_general x2 -> x0, matrix products: 24.5 us -> none  [the longest x1 15.4 us: evolve_memory(): jnp.einsum('bhvk,bhk->bhv', memory_arrays, unit_key, precision=HIGHEST)]
    pallas_call x1 -> x2, Pallas kernels: 20.3 us -> 43 us  [the longest x1 22.2 us: kernel_body(): pl.pallas_call(state_kernel, grid=(own // step,), out_shape=(jax.ShapeDty...]
    add x1 -> x0, other arithmetic: 10.6 us -> none  [evolve_memory(): memory_arrays * forget_lanes[:, :, None, :]]
    unnamed x23 -> x3, local copies, waits for them, and re-layouts: 9.83 us -> 1.38 us
    reshape x3 -> x0, local copies, waits for them, and re-layouts: 1.17 us -> none  [divide_lanes(): return channels.astype(jnp.float32).reshape(own, heads, LANE_WIDTH)]
where the time goes in v2:
time: 88.1 us; the launch traced here: 87.9 us
  Pallas kernels  85.2 us (97%)
  local copies, waits for them, and re-layouts  1.98 us (2%)
    pallas_call x1, Pallas kernels, kernel_body(): pl.pallas_call(functools.partial(ffn_kernel, ep, tp, FF_E), out_shape=jax...  42.2 us
    pallas_call x1, Pallas kernels, kernel_body(): pl.pallas_call(state_kernel, grid=(own // step,), out_shape=(jax.ShapeDty...  22.2 us
    pallas_call x1, Pallas kernels, kernel_body(): pl.pallas_call(functools.partial(project_kernel, ep, tp), out_shape=(per_...  20.8 us

profile of v2, /device:TPU:0, one launch (start us, length us, event | category | flops | bytes accessed | tf_op | source)
XLA Modules:
  0.0 87.9 jit_solution(13829683337261102340)
XLA Ops:
  0.6 0.0 copy-start
  0.6 20.8 %project.1 = (f32[16,16,64]{2,1,0:T(8,128)}, f32[16,16,64]{2,1,0:T(8,128)}, f32[16,16,64]{2,1,0:T(8,128)}, f32[16,16,64]{2,1,0:T(8,128)}, f32[16,16,64]{2,1,0:T(8,128)}, /*index=5*/f32[16,64]{1,0:T(8,128)}) custom-call(bf16[16,2048]{1,0:T(8,128)(2,1)} %x.3, f32[1,2048]{1,0:T(1,128)} %bitcast.15, bf16[1024,256]{1,0:T(8,128)(2,1)} %wq.1, ...), custom_call_target="tpu_custom_call" | custom-call | tf_op jit(solution)/shard_map/project/pallas_call | solution.py:551
  21.5 22.2 %state.1 = (f32[16,16,64,64]{3,2,1,0:T(8,128)}, f32[16,16,64]{2,1,0:T(8,128)}) custom-call(f32[16,16,64,64]{3,2,1,0:T(8,128)} %memory.1, f32[16,16,64]{2,1,0:T(8,128)} %get-tuple-element.10.query, f32[16,16,64]{2,1,0:T(8,128)} %get-tuple-element.11.key, f32[16,16,64]{2,1,0:T(8,128)} %get-tuple-element.12.value, f32[16,16,64]{2,1,0:T(8,128)} %get-tuple-element.13.decay, ...), custom_call_target="tpu_custom_call" | custom-call | tf_op jit(solution)/shard_map/state/pallas_call | solution.py:589
  43.6 0.0 copy-done
  43.6 0.6 reshape.27.cs
  44.2 42.2 %experts.1 = bf16[8,2048]{1,0:T(8,128)(2,1)} custom-call(f32[16,16,64]{2,1,0:T(8,128)} %get-tuple-element.16.read, bf16[16,2048]{1,0:T(8,128)(2,1)} %x.3, s32[2,16]{1,0:T(2,128)} %bitcast.20, bf16[2,16]{1,0:T(2,128)(2,1)} %bitcast.21, f32[1,2048]{1,0:T(1,128)} %bitcast.16, bf16[1,2048]{1,0:T(2,128)(2,1)} %reshape.27.cs, bf16[1024,256]{1,0:T(8,128)(2,1)} %wo_h.1, ...), custom_call_target="tpu_custom_call" | custom-call | tf_op jit(solution)/shard_map/experts/pallas_call | solution.py:601
  86.5 1.4 %copy.28 = bf16[8,2048]{1,0:T(8,128)(2,1)} copy(bf16[8,2048]{1,0:T(8,128)(2,1)} %experts.1) | data formatting | bytes 65536
Async XLA Ops:
  0.6 43.0 %copy-start = (bf16[2048]{0:T(1024)(128)(2,1)S(1)}, bf16[2048]{0:T(1024)(128)(2,1)}, u32[]{:S(2)}) copy-start(bf16[2048]{0:T(1024)(128)(2,1)} %param.49) | copy-start | bytes 12292

commit v3 on v2

--- a/solution.py
+++ b/solution.py
@@ -189,7 +189,7 @@
                 fn(lax.rem(me + far, ep), lax.rem(core + side, tp))
 
 
-def _meet(ep, tp):
+def _greet(ep, tp):
     barrier = pltpu.get_barrier_semaphore()
     _others(
         ep,
@@ -198,7 +198,10 @@
             barrier, inc=1, device_id={"ep": e, "tp": t}, device_id_type=MESH
         ),
     )
-    pl.semaphore_wait(barrier, ep * tp - 1)
+
+
+def _met(ep, tp):
+    pl.semaphore_wait(pltpu.get_barrier_semaphore(), ep * tp - 1)
 
 
 def _remote(src, dst, send, recv, e, t):
@@ -223,25 +226,48 @@
         ref[:, first + h, :] = channels[:, h * LANE_WIDTH : (h + 1) * LANE_WIDTH]
 
 
-def state_kernel(memory, query, key, value, decay, rate, lane_gain, reward, after, read, flip):
+def split_dot(left, right, dims):
+    tops = [f.astype(jnp.bfloat16) for f in (left, right)]
+    rests = [(f - h.astype(jnp.float32)).astype(jnp.bfloat16) for f, h in zip((left, right), tops)]
+    pairs = ((tops[0], rests[1]), (rests[0], tops[1]), (tops[0], tops[1]))
+    return sum(
+        lax.dot_general(a, b, (dims, ((), ())), preferred_element_type=jnp.float32)
+        for a, b in pairs
+    )
+
+
+def state_kernel(
+    memory, query, key, value, decay, rate, lane_gain, reward, after, read, flip, probes, moves
+):
     count, heads = query.shape[0], query.shape[1]
     lane = lax.broadcasted_iota(jnp.int32, (LANE_WIDTH, 128), 1)
+    turn = lax.rem(lane, heads)
+    chunk = math.gcd(heads, 4)
 
     def sequence(b, carry):
         q, k, v, d, r = query[b], key[b], value[b], decay[b], rate[b]
         unit = k * lax.rsqrt(jnp.sum(k * k, axis=-1, keepdims=True) + 1.0)
         scaled, pulled, seen = k * r, unit * r, d * q
-        flip[0:heads] = v
+        flip[2 * heads : 3 * heads] = v
+        probes[0:heads] = unit
+        probes[heads : 2 * heads] = seen
+        moves[0:heads] = -pulled
+        moves[2 * heads : 3 * heads] = scaled
         value_cols = flip[...].T
         found = jnp.zeros((LANE_WIDTH, 128), jnp.float32)
-        for h in range(heads):
-            one = slice(h, h + 1)
-            m = memory[b, h]
-            removal = jnp.sum(m * unit[one], axis=-1, keepdims=True)
-            kept = jnp.sum(m * seen[one], axis=-1, keepdims=True)
-            after[b, h] = m * d[one] - removal * pulled[one] + value_cols[:, one] * scaled[one]
-            found = jnp.where(lane == h, removal, found)
-            found = jnp.where(lane == heads + h, kept, found)
+        for first in range(0, heads, chunk):
+            m = memory[b, first : first + chunk]
+            sums = split_dot(m.reshape(chunk * LANE_WIDTH, LANE_WIDTH), probes[...], ((1,), (1,)))
+            factors = []
+            for i in range(chunk):
+                both = sums[i * LANE_WIDTH : (i + 1) * LANE_WIDTH]
+                both = jnp.where(lane < 2 * heads, both, value_cols)
+                factors.append(jnp.where(turn == first + i, both, 0.0))
+                found = found + factors[-1]
+            change = split_dot(jnp.concatenate(factors, axis=0), moves[...], ((1,), (0,)))
+            for i in range(chunk):
+                h = first + i
+                after[b, h] = m[i] * d[h : h + 1] + change[i * LANE_WIDTH : (i + 1) * LANE_WIDTH]
         rows = found.T
         out = (
             rows[heads : 2 * heads]
@@ -254,7 +280,8 @@
         read[b] = centred * level * lane_gain[...] + extra
         return carry
 
-    flip[...] = jnp.zeros_like(flip)
+    for ref in (flip, probes, moves):
+        ref[...] = jnp.zeros_like(ref)
     lax.fori_loop(0, count, sequence, 0)
 
 
@@ -265,6 +292,7 @@
 ):
     me, core = lax.axis_index("ep"), lax.axis_index("tp")
     group = ep // tp
+    _greet(ep, tp)
     loads = [pltpu.make_async_copy(ref, w.at[i], wsem.at[i]) for i, ref in enumerate((wq, wk, wv))]
     for load in loads:
         load.start()
@@ -274,7 +302,7 @@
     normed = (rms_norm(values, gain[...])).astype(jnp.bfloat16)
     for i in range(tp):
         halves[i] = normed[:, i * half : (i + 1) * half]
-    _meet(ep, tp)
+    _met(ep, tp)
     sends = []
     for far in range(1, ep):
         e = lax.rem(me + far, ep)
@@ -350,6 +378,7 @@
     group = ep // tp
     own, width = x.shape
     cols = wo.shape[1]
+    _greet(ep, tp)
     loads = [
         pltpu.make_async_copy(a, b, wsem.at[i])
         for i, (a, b) in enumerate(
@@ -365,12 +394,12 @@
         routes = routes + jnp.where(
             ids_cols[:, k : k + 1] == lane, coef_cols[:, k : k + 1], 0.0
         )
-    share[me] = routes
+    share[me] = routes.astype(jnp.bfloat16)
     pack = 128 // LANE_WIDTH
     for h in range(0, read.shape[1], pack):
         joined = jnp.concatenate([read[:, h + i, :] for i in range(pack)], axis=-1)
         att[:, h * LANE_WIDTH : h * LANE_WIDTH + 128] = joined.astype(jnp.bfloat16)
-    _meet(ep, tp)
+    _met(ep, tp)
     sends = []
 
     def push(*args):
@@ -380,10 +409,20 @@
     for far in range(1, ep):
         e = lax.rem(me + far, ep)
         push(att, att_all.at[me], s_att.at[far], r_att.at[me], e, core)
+    side = me // group
+    blocks = []
     for far in range(1, ep):
         e = lax.rem(me + far, ep)
         block = x.at[:, pl.ds(pl.multiple_of(e * cols, cols), cols)]
-        push(block, xcol.at[me], s_x.at[far], r_x.at[me], e, core)
+        blocks.append(_remote(block, xcol.at[me], s_x.at[far], r_x.at[me], e, core))
+
+    @pl.when(side == core)
+    def _():
+        for copy in blocks:
+            copy.start()
+
+    for far in range(1, ep):
+        e = lax.rem(me + far, ep)
         push(share.at[me], share.at[me], s_sh.at[far], r_sh.at[me], e, core)
     att_all[me] = att[...]
     xcol[me] = x[:, pl.ds(pl.multiple_of(me * cols, cols), cols)]
@@ -401,9 +440,13 @@
     ).astype(jnp.bfloat16)
     pbuf[...] = done.reshape(tp, group * own, cols)
     push(pbuf.at[mate], psib, s_p, r_p, me, mate)
-    for far in range(1, ep):
-        e = lax.rem(me + far, ep)
-        arrive(xcol.at[e], r_x.at[e])
+    for j in range(group):
+        e = core * group + j
+
+        @pl.when(e != me)
+        def _():
+            arrive(xcol.at[e], r_x.at[e])
+
     arrive(psib, r_p)
     mixed = (pbuf[core].astype(jnp.float32) + psib[...].astype(jnp.float32)).astype(jnp.bfloat16)
     held = xcol[pl.ds(core * group, group)].reshape(group * own, cols).astype(jnp.float32)
@@ -439,7 +482,7 @@
         e = lax.rem(me + far, ep)
         arrive(share.at[e], r_sh.at[e])
     expert = (me * tp + core) * wg.shape[1] // expert_cols
-    table = share[...].reshape(rows, 128)
+    table = share[...].astype(jnp.float32).reshape(rows, 128)
     picked = lax.broadcasted_iota(jnp.int32, (rows, 128), 1) == expert
     weight = jnp.sum(jnp.where(picked, table, 0.0), axis=-1, keepdims=True)
     for i in (1, 2):
@@ -467,8 +510,8 @@
         y = weight * jnp.dot(hid[...], wd[:, at], preferred_element_type=jnp.float32)
         y = y + branch_scale * jnp.dot(chid[...], cd[:, at], preferred_element_type=jnp.float32)
         y = y.reshape(ep, tp, last, piece)
-        for side in range(tp):
-            sibout[n, side] = y[:, side].astype(jnp.bfloat16)
+        for k in range(tp):
+            sibout[n, k] = y[:, k].astype(jnp.bfloat16)
         push(sibout.at[n, mate], sibin.at[n], s_sib.at[n], r_sib.at[n], me, mate)
     for n in range(pieces):
         arrive(sibin.at[n], r_sib.at[n])
@@ -494,11 +537,18 @@
     for send in sends:
         send.wait_send()
 
+    @pl.when(side == core)
+    def _():
+        for copy in blocks:
+            copy.wait_send()
+
 
 def layer(*blocks):
     own = blocks[0].shape[0]
     cols, hidden = blocks[9].shape[1], blocks[18].shape[1]
+    heads = blocks[17].shape[0]
     tiles = cols % 128 == 0 and hidden % 256 == 0 and own % 16 == 0
+    tiles = tiles and heads % 8 == 0 and 128 % heads == 0 and heads <= 32
     heads_match = lax.axis_size("ep") % lax.axis_size("tp") == 0 and lax.axis_size("tp") == 2
     weights = sum(2 * w.size for w in blocks[18:24])
     rows = own * lax.axis_size("ep")
@@ -592,7 +642,7 @@
         out_shape=(jax.ShapeDtypeStruct(memory_arrays.shape, f32), per_head),
         in_specs=[memory_spec] + [lane_spec] * 5 + [gain_spec] * 2,
         out_specs=(memory_spec, lane_spec),
-        scratch_shapes=[pltpu.VMEM((128, LANE_WIDTH), f32)],
+        scratch_shapes=[pltpu.VMEM((128, LANE_WIDTH), f32)] * 3,
         name="state",
     )(memory_arrays, *lanes, lane_gain, instant_reward)
     rows, hidden, dense = ep * own, specialist_switch.shape[1], common_activator.shape[1]
@@ -607,7 +657,7 @@
             pltpu.VMEM((own, half), bf16),
             pltpu.VMEM((ep, own, half), bf16),
             pltpu.VMEM((ep, own, cols), bf16),
-            pltpu.VMEM((ep, own, 128), f32),
+            pltpu.VMEM((ep, own, 128), bf16),
             pltpu.VMEM((half, cols), bf16),
             pltpu.VMEM((width, hidden), bf16),
             pltpu.VMEM((width, hidden), bf16),

time: 88.1 us -> 84.7 us (0.961)
  Pallas kernels: 85.2 us -> 81.8 us
    pallas_call x1, Pallas kernels: 22.2 us -> 20 us  [kernel_body(): pl.pallas_call(state_kernel, grid=(own // step,), out_shape=(jax.ShapeDty...]
    pallas_call x1, Pallas kernels: 42.2 us -> 41.1 us  [kernel_body(): pl.pallas_call(functools.partial(ffn_kernel, ep, tp, FF_E), out_shape=jax...]
where the time goes in v3:
time: 84.7 us; the launch traced here: 84.4 us
  Pallas kernels  81.8 us (97%)
  local copies, waits for them, and re-layouts  1.98 us (2%)
    pallas_call x1, Pallas kernels, kernel_body(): pl.pallas_call(functools.partial(ffn_kernel, ep, tp, FF_E), out_shape=jax...  41.1 us
    pallas_call x1, Pallas kernels, kernel_body(): pl.pallas_call(functools.partial(project_kernel, ep, tp), out_shape=(per_...  20.6 us
    pallas_call x1, Pallas kernels, kernel_body(): pl.pallas_call(state_kernel, grid=(own // step,), out_shape=(jax.ShapeDty...  20 us

profile of v3, /device:TPU:0, one launch (start us, length us, event | category | flops | bytes accessed | tf_op | source)
XLA Modules:
  0.0 84.4 jit_solution(1838457645057914065)
XLA Ops:
  0.6 0.0 copy-start
  0.6 20.6 %project.1 = (f32[16,16,64]{2,1,0:T(8,128)}, f32[16,16,64]{2,1,0:T(8,128)}, f32[16,16,64]{2,1,0:T(8,128)}, f32[16,16,64]{2,1,0:T(8,128)}, f32[16,16,64]{2,1,0:T(8,128)}, /*index=5*/f32[16,64]{1,0:T(8,128)}) custom-call(bf16[16,2048]{1,0:T(8,128)(2,1)} %x.3, f32[1,2048]{1,0:T(1,128)} %bitcast.15, bf16[1024,256]{1,0:T(8,128)(2,1)} %wq.1, ...), custom_call_target="tpu_custom_call" | custom-call | tf_op jit(solution)/shard_map/project/pallas_call | solution.py:601
  21.3 20.0 %state.1 = (f32[16,16,64,64]{3,2,1,0:T(8,128)}, f32[16,16,64]{2,1,0:T(8,128)}) custom-call(f32[16,16,64,64]{3,2,1,0:T(8,128)} %memory.1, f32[16,16,64]{2,1,0:T(8,128)} %get-tuple-element.10.query, f32[16,16,64]{2,1,0:T(8,128)} %get-tuple-element.11.key, f32[16,16,64]{2,1,0:T(8,128)} %get-tuple-element.12.value, f32[16,16,64]{2,1,0:T(8,128)} %get-tuple-element.13.decay, ...), custom_call_target="tpu_custom_call" | custom-call | tf_op jit(solution)/shard_map/state/pallas_call | solution.py:639
  41.3 0.0 copy-done
  41.3 0.6 reshape.27.cs
  41.9 41.1 %experts.1 = bf16[8,2048]{1,0:T(8,128)(2,1)} custom-call(f32[16,16,64]{2,1,0:T(8,128)} %get-tuple-element.16.read, bf16[16,2048]{1,0:T(8,128)(2,1)} %x.3, s32[2,16]{1,0:T(2,128)} %bitcast.20, bf16[2,16]{1,0:T(2,128)(2,1)} %bitcast.21, f32[1,2048]{1,0:T(1,128)} %bitcast.16, bf16[1,2048]{1,0:T(2,128)(2,1)} %reshape.27.cs, bf16[1024,256]{1,0:T(8,128)(2,1)} %wo_h.1, ...), custom_call_target="tpu_custom_call" | custom-call | tf_op jit(solution)/shard_map/experts/pallas_call | solution.py:651
  83.1 1.4 %copy.28 = bf16[8,2048]{1,0:T(8,128)(2,1)} copy(bf16[8,2048]{1,0:T(8,128)(2,1)} %experts.1) | data formatting | bytes 65536
Async XLA Ops:
  0.6 40.7 %copy-start = (bf16[2048]{0:T(1024)(128)(2,1)S(1)}, bf16[2048]{0:T(1024)(128)(2,1)}, u32[]{:S(2)}) copy-start(bf16[2048]{0:T(1024)(128)(2,1)} %param.49) | copy-start | bytes 12292

commit v4 on v3

--- a/solution.py
+++ b/solution.py
@@ -226,13 +226,12 @@
         ref[:, first + h, :] = channels[:, h * LANE_WIDTH : (h + 1) * LANE_WIDTH]
 
 
-def split_dot(left, right, dims):
-    tops = [f.astype(jnp.bfloat16) for f in (left, right)]
-    rests = [(f - h.astype(jnp.float32)).astype(jnp.bfloat16) for f, h in zip((left, right), tops)]
-    pairs = ((tops[0], rests[1]), (rests[0], tops[1]), (tops[0], tops[1]))
-    return sum(
-        lax.dot_general(a, b, (dims, ((), ())), preferred_element_type=jnp.float32)
-        for a, b in pairs
+def round_dot(left, right, dims):
+    return lax.dot_general(
+        left.astype(jnp.bfloat16),
+        right.astype(jnp.bfloat16),
+        (dims, ((), ())),
+        preferred_element_type=jnp.float32,
     )
 
 
@@ -244,27 +243,27 @@
     turn = lax.rem(lane, heads)
     chunk = math.gcd(heads, 4)
 
-    def sequence(b, carry):
+    def sequence(b):
         q, k, v, d, r = query[b], key[b], value[b], decay[b], rate[b]
         unit = k * lax.rsqrt(jnp.sum(k * k, axis=-1, keepdims=True) + 1.0)
         scaled, pulled, seen = k * r, unit * r, d * q
-        flip[2 * heads : 3 * heads] = v
-        probes[0:heads] = unit
-        probes[heads : 2 * heads] = seen
-        moves[0:heads] = -pulled
-        moves[2 * heads : 3 * heads] = scaled
-        value_cols = flip[...].T
+        flip[b, 2 * heads : 3 * heads] = v
+        probes[b, 0:heads] = unit
+        probes[b, heads : 2 * heads] = seen
+        moves[b, 0:heads] = -pulled
+        moves[b, 2 * heads : 3 * heads] = scaled
+        value_cols = flip[b].T
         found = jnp.zeros((LANE_WIDTH, 128), jnp.float32)
         for first in range(0, heads, chunk):
             m = memory[b, first : first + chunk]
-            sums = split_dot(m.reshape(chunk * LANE_WIDTH, LANE_WIDTH), probes[...], ((1,), (1,)))
+            sums = round_dot(m.reshape(chunk * LANE_WIDTH, LANE_WIDTH), probes[b], ((1,), (1,)))
             factors = []
             for i in range(chunk):
                 both = sums[i * LANE_WIDTH : (i + 1) * LANE_WIDTH]
                 both = jnp.where(lane < 2 * heads, both, value_cols)
                 factors.append(jnp.where(turn == first + i, both, 0.0))
                 found = found + factors[-1]
-            change = split_dot(jnp.concatenate(factors, axis=0), moves[...], ((1,), (0,)))
+            change = round_dot(jnp.concatenate(factors, axis=0), moves[b], ((1,), (0,)))
             for i in range(chunk):
                 h = first + i
                 after[b, h] = m[i] * d[h : h + 1] + change[i * LANE_WIDTH : (i + 1) * LANE_WIDTH]
@@ -278,11 +277,11 @@
         level = lax.rsqrt(jnp.mean(centred * centred, axis=-1, keepdims=True) + GROUP_EPS)
         extra = jnp.sum(q * scaled * reward[...], axis=-1, keepdims=True) * v
         read[b] = centred * level * lane_gain[...] + extra
-        return carry
 
     for ref in (flip, probes, moves):
         ref[...] = jnp.zeros_like(ref)
-    lax.fori_loop(0, count, sequence, 0)
+    for b in range(count):
+        sequence(b)
 
 
 def project_kernel(
@@ -642,7 +641,7 @@
         out_shape=(jax.ShapeDtypeStruct(memory_arrays.shape, f32), per_head),
         in_specs=[memory_spec] + [lane_spec] * 5 + [gain_spec] * 2,
         out_specs=(memory_spec, lane_spec),
-        scratch_shapes=[pltpu.VMEM((128, LANE_WIDTH), f32)] * 3,
+        scratch_shapes=[pltpu.VMEM((step, 128, LANE_WIDTH), f32)] * 3,
         name="state",
     )(memory_arrays, *lanes, lane_gain, instant_reward)
     rows, hidden, dense = ep * own, specialist_switch.shape[1], common_activator.shape[1]

time: 84.7 us -> 76.5 us (0.903)
  Pallas kernels: 81.8 us -> 73.4 us
    pallas_call x1, Pallas kernels: 20 us -> 11.7 us  [kernel_body(): pl.pallas_call(state_kernel, grid=(own // step,), out_shape=(jax.ShapeDty...]
where the time goes in v4:
time: 76.5 us; the launch traced here: 76.1 us
  Pallas kernels  73.4 us (96%)
  local copies, waits for them, and re-layouts  1.98 us (3%)
    pallas_call x1, Pallas kernels, kernel_body(): pl.pallas_call(functools.partial(ffn_kernel, ep, tp, FF_E), out_shape=jax...  41.1 us
    pallas_call x1, Pallas kernels, kernel_body(): pl.pallas_call(functools.partial(project_kernel, ep, tp), out_shape=(per_...  20.6 us
    pallas_call x1, Pallas kernels, kernel_body(): pl.pallas_call(state_kernel, grid=(own // step,), out_shape=(jax.ShapeDty...  11.7 us

profile of v4, /device:TPU:0, one launch (start us, length us, event | category | flops | bytes accessed | tf_op | source)
XLA Modules:
  0.0 76.1 jit_solution(1225130195691674703)
XLA Ops:
  0.6 0.0 copy-start
  0.6 20.6 %project.1 = (f32[16,16,64]{2,1,0:T(8,128)}, f32[16,16,64]{2,1,0:T(8,128)}, f32[16,16,64]{2,1,0:T(8,128)}, f32[16,16,64]{2,1,0:T(8,128)}, f32[16,16,64]{2,1,0:T(8,128)}, /*index=5*/f32[16,64]{1,0:T(8,128)}) custom-call(bf16[16,2048]{1,0:T(8,128)(2,1)} %x.3, f32[1,2048]{1,0:T(1,128)} %bitcast.15, bf16[1024,256]{1,0:T(8,128)(2,1)} %wq.1, ...), custom_call_target="tpu_custom_call" | custom-call | tf_op jit(solution)/shard_map/project/pallas_call | solution.py:600
  21.3 11.7 %state.1 = (f32[16,16,64,64]{3,2,1,0:T(8,128)}, f32[16,16,64]{2,1,0:T(8,128)}) custom-call(f32[16,16,64,64]{3,2,1,0:T(8,128)} %memory.1, f32[16,16,64]{2,1,0:T(8,128)} %get-tuple-element.10.query, f32[16,16,64]{2,1,0:T(8,128)} %get-tuple-element.11.key, f32[16,16,64]{2,1,0:T(8,128)} %get-tuple-element.12.value, f32[16,16,64]{2,1,0:T(8,128)} %get-tuple-element.13.decay, ...), custom_call_target="tpu_custom_call" | custom-call | tf_op jit(solution)/shard_map/state/pallas_call | solution.py:638
  33.0 0.0 copy-done
  33.0 0.6 reshape.27.cs
  33.6 41.1 %experts.1 = bf16[8,2048]{1,0:T(8,128)(2,1)} custom-call(f32[16,16,64]{2,1,0:T(8,128)} %get-tuple-element.16.read, bf16[16,2048]{1,0:T(8,128)(2,1)} %x.3, s32[2,16]{1,0:T(2,128)} %bitcast.20, bf16[2,16]{1,0:T(2,128)(2,1)} %bitcast.21, f32[1,2048]{1,0:T(1,128)} %bitcast.16, bf16[1,2048]{1,0:T(2,128)(2,1)} %reshape.27.cs, bf16[1024,256]{1,0:T(8,128)(2,1)} %wo_h.1, ...), custom_call_target="tpu_custom_call" | custom-call | tf_op jit(solution)/shard_map/experts/pallas_call | solution.py:650
  74.7 1.4 %copy.28 = bf16[8,2048]{1,0:T(8,128)(2,1)} copy(bf16[8,2048]{1,0:T(8,128)(2,1)} %experts.1) | data formatting | bytes 65536
Async XLA Ops:
  0.6 32.3 %copy-start = (bf16[2048]{0:T(1024)(128)(2,1)S(1)}, bf16[2048]{0:T(1024)(128)(2,1)}, u32[]{:S(2)}) copy-start(bf16[2048]{0:T(1024)(128)(2,1)} %param.49) | copy-start | bytes 12292
